TPU v7x, 256 devices: a whole 4x4x8 slice. The times are simulated.
256 devices in a mesh: sp: 64 (over z, x, core), tp: 4 (over y).
Axes of the slice: x: 4, y: 4, z: 8, core: 2. Of those that a mesh axis runs over, the one named last changes fastest.
Arguments:
- residual_in: bfloat16 [65536, 2048], P(('sp', 'tp')), may hold values from -6 to 6
- gate_outer: bfloat16 [65536, 1024], P('sp', 'tp'), may hold values from -6 to 6
- gate_inner: bfloat16 [65536, 1024], P('sp', 'tp'), may hold values from -6 to 6
- conv_input: bfloat16 [65536, 1024], P('sp', 'tp'), may hold values from -6 to 6
- conv_taps: bfloat16 [3, 1024], P(None, 'tp'), may hold values from -5 to 5
- norm_gain: bfloat16 [1024], P('tp'), may hold values from 0.099609375 to 1.8984375
- out_weight: bfloat16 [1024, 2048], P('tp'), may hold values from -0.1875 to 0.1875
- moe_gain: bfloat16 [2048], replicated, may hold values from 0.099609375 to 1.8984375
- expert_ids: int32 [65536, 2], P(('sp', 'tp')), may hold values from 0 to 63, all different within a row; in each aligned block of 256 rows (0 to 255, 256 to 511, ...) at most 16 rows name the same one
- group_prob: float32 [65536], P(('sp', 'tp')), may hold values from 0.3 to 1
- route_prob: float32 [65536, 2], P(('sp', 'tp')), may hold values from 0.1 to 1
- expert_gate: bfloat16 [64, 2048, 512], P('sp'), may hold values from -0.125 to 0.125
- expert_up: bfloat16 [64, 2048, 512], P('sp'), may hold values from -0.125 to 0.125
- expert_down: bfloat16 [64, 512, 2048], P('sp'), may hold values from -0.25 to 0.25
Outputs:
- layer_out: bfloat16 [65536, 2048], P(('sp', 'tp'))
Inputs may be any that keep to these rules, and one draw needn't show every extreme that they name: `expert_ids`: each row names 2 different experts. Within the rows of one device (aligned blocks of 256 rows) no expert is named more than 16 times.
All inputs are finite; a program needn't handle non-finite values.
Results may differ from a plain program's by a relative error of at most 0.0075.
Values may be sent and summed in bfloat16 or wider, within the bound.
A program may use at most 64 MiB of HBM per device.

v0:
```python
import jax
import jax.numpy as jnp
from jax import lax
from jax.sharding import PartitionSpec as P

EPSILON = 1e-06


def from_behind(shard, axis, by):
    devices = lax.axis_size(axis)
    pairs = [(i, i + by) for i in range(devices) if 0 <= i + by < devices]
    return lax.ppermute(shard, axis, pairs)


def rms_norm(values, gain):
    floats = values.astype(jnp.float32)
    factor = lax.rsqrt(jnp.mean(floats * floats, axis=-1, keepdims=True) + EPSILON)
    return floats * factor * gain.astype(jnp.float32)


def body(
    residual_in,
    gate_outer,
    gate_inner,
    conv_input,
    conv_taps,
    norm_gain,
    out_weight,
    moe_gain,
    expert_ids,
    group_prob,
    route_prob,
    expert_gate,
    expert_up,
    expert_down,
):
    seq_rows, channels = conv_input.shape
    taps_count = conv_taps.shape[0]
    inner = gate_inner.astype(jnp.float32) * conv_input.astype(jnp.float32)
    earlier = from_behind(inner[seq_rows - (taps_count - 1) :], "sp", 1)
    padded = jnp.concatenate([earlier, inner], axis=0)
    tap_f = conv_taps.astype(jnp.float32)
    filtered = jnp.zeros((seq_rows, channels), jnp.float32)
    for offset in range(taps_count):
        filtered = filtered + tap_f[offset][None, :] * padded[offset : offset + seq_rows]
    mixed_out = (gate_outer.astype(jnp.float32) * filtered).astype(jnp.bfloat16)
    gathered = lax.all_to_all(mixed_out, "tp", split_axis=0, concat_axis=1, tiled=True)
    full_weight, full_gain = (
        lax.all_gather(out_weight, "tp", axis=0, tiled=True),
        lax.all_gather(norm_gain, "tp", axis=0, tiled=True),
    )
    normed = rms_norm(gathered, full_gain).astype(jnp.bfloat16)
    projected = jnp.dot(normed, full_weight, preferred_element_type=jnp.float32)
    residual = (residual_in.astype(jnp.float32) + projected).astype(jnp.bfloat16)
    routed_in = rms_norm(residual, moe_gain).astype(jnp.bfloat16)
    tok_rows, width = routed_in.shape
    top_count = expert_ids.shape[1]
    local_count = expert_gate.shape[0]
    group_count = lax.axis_size("sp")
    experts_all = local_count * group_count
    capacity = 2 * tok_rows * top_count // experts_all
    slots = tok_rows * top_count
    flat_e = expert_ids.reshape(-1)
    one_hot = (flat_e[:, None] == jnp.arange(experts_all, dtype=jnp.int32)[None, :]).astype(
        jnp.int32
    )
    slot_rank = jnp.sum((jnp.cumsum(one_hot, axis=0) - 1) * one_hot, axis=1)
    owner_dev = flat_e // local_count
    local_slot = flat_e % local_count
    position = (local_slot * group_count + owner_dev) * capacity + slot_rank
    source_slot = (
        jnp.full((experts_all * capacity,), slots, jnp.int32)
        .at[position]
        .set(jnp.arange(slots, dtype=jnp.int32))
    )
    rows_pad = jnp.concatenate([routed_in, jnp.zeros((1, width), jnp.bfloat16)], axis=0)
    outgoing = rows_pad[source_slot // top_count].reshape(local_count, group_count, capacity, width)
    arrived = lax.all_to_all(outgoing, "sp", split_axis=1, concat_axis=1, tiled=True)
    gate_act = jnp.einsum(
        "esrd,edf->esrf", arrived, expert_gate, preferred_element_type=jnp.float32
    )
    up_act = jnp.einsum("esrd,edf->esrf", arrived, expert_up, preferred_element_type=jnp.float32)
    hidden = (jax.nn.silu(gate_act) * up_act).astype(jnp.bfloat16)
    result = jnp.einsum(
        "esrf,efd->esrd", hidden, expert_down, preferred_element_type=jnp.float32
    ).astype(jnp.bfloat16)
    returned = lax.all_to_all(result, "sp", split_axis=1, concat_axis=1, tiled=True)
    slot_out = returned.reshape(-1, width)[position].reshape(tok_rows, top_count, width)
    weights = group_prob[:, None] * route_prob / jnp.sum(route_prob, axis=1, keepdims=True)
    expert_sum = jnp.sum(slot_out.astype(jnp.float32) * weights[:, :, None], axis=1)
    return (residual.astype(jnp.float32) + expert_sum).astype(jnp.bfloat16)


def solution(mesh):
    in_specs = (
        P(("sp", "tp"), None),
        P("sp", "tp"),
        P("sp", "tp"),
        P("sp", "tp"),
        P(None, "tp"),
        P("tp"),
        P("tp", None),
        P(),
        P(("sp", "tp"), None),
        P(("sp", "tp")),
        P(("sp", "tp"), None),
        P("sp", None, None),
        P("sp", None, None),
        P("sp", None, None),
    )
    out_specs = P(("sp", "tp"), None)
    return jax.shard_map(body, mesh=mesh, in_specs=in_specs, out_specs=out_specs, check_vma=False)
```

profile of v0, /device:TPU:1, one launch (start us, length us, event | category | flops | bytes accessed | tf_op | source)
XLA Modules:
  0.0 334.6 jit_solution(17748182596416122300)
XLA Ops:
  6.5 0.0 copy-start
  6.5 0.0 copy-start.4
  6.5 0.0 copy-start.6
  6.5 0.0 copy-start.10
  6.5 0.0 copy-start.7
  6.5 0.0 all-gather.3.cloned.1.call-start
  6.6 0.7 all-gather.3.cloned.1.call-update
  7.3 1.3 convert_multiply_fusion.3
  8.6 4.5 %collective-permute-start = (f32[2,256]{1,0:T(2,128)S(1)}, f32[2,256]{1,0:T(2,128)S(1)}, u32[]{:S(2)}, u32[]{:S(2)}) collective-permute-start(f32[2,256]{1,0:T(2,128)S(1)} %slice.37), channel_id=1, source_target_pairs={{0,4},{4,8},{8,12},{12,16},{16,20},{20,24},{24,28},{28,32},{32,36}... | collective-permute-start | bytes 6152 | tf_op jit(solution)/shard_map/ppermute | solution.py:12
  13.1 0.0 copy-done.4
  13.1 0.1 copy.29
  13.3 0.1 eq.31
  13.4 0.1 eq.27
  13.6 1.2 reduce-window.6
  14.8 0.2 slice_reduce_fusion
  15.1 0.0 copy-done.6
  15.1 0.1 fusion.32
  15.2 0.0 copy-done.10
  15.2 8.0 %all-gather = bf16[4,1,256]{2,1,0:T(2,128)(2,1)S(1)} all-gather(bf16[1,1,256]{2,1,0:T(2,128)(2,1)S(1)} %reshape.144), channel_id=1, replica_groups=mesh['sp'=64,'tp'=4] {'tp'}, dimensions={0}, use_global_device_ids=true | all-gather | bytes 2560 | tf_op jit(solution)/shard_map/all_gather | solution.py:50
  23.2 0.0 copy-done.7
  23.2 0.1 copy.28
  23.4 0.1 mul.147
  23.5 0.0 collective-permute-done
  23.5 2.3 fusion.25
  25.8 3.5 %all-to-all-start = ((bf16[4,256,256]{2,1,0:T(8,128)(2,1)}), bf16[4,256,256]{2,1,0:T(8,128)(2,1)S(1)}, u32[]{:S(2)}, u32[]{:S(2)}) async-start(bf16[4,256,256]{2,1,0:T(8,128)(2,1)} %bitcast.66), calls=%async_computation | async-start | bytes 1048576 | tf_op jit(solution)/shard_map/all_to_all | solution.py:47
  29.3 2.4 scatter_custom_fusion
  31.8 12.9 %all-to-all-done = bf16[4,256,256]{2,1,0:T(8,128)(2,1)S(1)} async-done(((bf16[4,256,256]{2,1,0:T(8,128)(2,1)}), bf16[4,256,256]{2,1,0:T(8,128)(2,1)S(1)}, u32[]{:S(2)}, u32[]{:S(2)}) %all-to-all-start) | async-done | bytes 524320 | tf_op jit(solution)/shard_map/all_to_all | solution.py:47
  44.7 1.1 convert_bitcast_fusion.1
  45.7 2.5 copy.27
  48.3 0.2 fusion.26
  48.5 1.4 fusion.29
  49.9 19.3 %all-gather.3.cloned.1.call-done = bf16[1024,2048]{1,0:T(8,128)(2,1)} async-done(((bf16[256,2048]{1,0:T(8,128)(2,1)}), bf16[1024,2048]{1,0:T(8,128)(2,1)}) %all-gather.3.cloned.1.call-update) | async-done | bytes 4194320 | tf_op jit(solution)/shard_map/all_gather | solution.py:49
  69.2 3.9 %fusion.5 = (f32[256]{0:T(256)S(1)}, bf16[256,2048]{1,0:T(8,128)(2,1)S(1)}) fusion(bf16[256,1024]{0,1:T(8,128)(2,1)S(1)} %fusion.29, bf16[1024,2048]{1,0:T(8,128)(2,1)} %all-gather.3.cloned.1.call-done, bf16[256,2048]{1,0:T(8,128)(2,1)} %param.14), kind=kOutput, calls=%fused_computation.14 | convolution fusion | flops 1076887296 | bytes 6816768 | tf_op jit(solution)/shard_map/dot_general | solution.py:53
  73.1 0.0 copy-start.2
  73.1 1.0 copy-done.2
  74.1 0.3 fusion.7
  74.4 0.1 concatenate.7
  74.5 6.0 %gather_fusion = bf16[1024,2048]{1,0:T(8,128)(2,1)} fusion(bf16[257,2048]{1,0:T(8,128)(2,1)S(1)} %concatenate.7, s32[1024]{0:T(1024)S(1)} %fusion.35), kind=kCustom, calls=%fused_computation | custom fusion | bytes 8392704 | tf_op jit(solution)/shard_map/gather | solution.py:77
  80.5 0.0 copy-start.9
  80.5 105.6 %all_to_all.23 = bf16[1,64,16,2048]{3,2,0,1:T(8,128)(2,1)S(1)} all-to-all(bf16[1,64,16,2048]{3,2,0,1:T(8,128)(2,1)} %bitcast.65), channel_id=1, replica_groups=mesh['sp'=64,'tp'=4] {'sp'}, dimensions={1} | all-to-all | bytes 8388608 | tf_op jit(solution)/shard_map/all_to_all | solution.py:78
  186.1 0.0 copy-start.1
  186.1 2.0 copy-done.1
  188.1 0.0 copy-done.9
  188.1 3.7 %fusion.2 = f32[64,16,512]{2,1,0:T(8,128)} fusion(bf16[1,64,16,2048]{3,2,0,1:T(8,128)(2,1)S(1)} %all_to_all.23, bf16[1,2048,512]{2,1,0:T(8,128)(2,1)S(1)} %copy-done.9), kind=kOutput, calls=%fused_computation.5 | convolution fusion | flops 2147483648 | bytes 8388608 | tf_op jit(solution)/shard_map/esrd,edf->esrf/dot_general | solution.py:79
  191.8 0.0 copy-done
  191.8 10.0 %convert_bitcast_fusion = bf16[1,64,16,2048]{3,2,0,1:T(8,128)(2,1)} fusion(bf16[1,512,2048]{2,1,0:T(8,128)(2,1)S(1)} %copy-done, f32[64,16,512]{2,1,0:T(8,128)} %fusion.2, bf16[1,2048,512]{2,1,0:T(8,128)(2,1)} %param.26, bf16[1,64,16,2048]{3,2,0,1:T(8,128)(2,1)} %copy-done.1), kind=kOutput, calls=%fused_computation.8 | convolution fusion | flops 4300210176 | bytes 14680064 | tf_op jit(solution)/shard_map/esrf,efd->esrd/dot_general | solution.py:84
  201.8 0.0 copy-start.5
  201.8 0.0 copy-start.8
  201.8 7.5 %all-to-all-start.2 = ((bf16[1,64,16,2048]{3,2,0,1:T(8,128)(2,1)}), bf16[1,64,16,2048]{3,2,0,1:T(8,128)(2,1)}, u32[]{:S(2)}, u32[]{:S(2)}) async-start(bf16[1,64,16,2048]{3,2,0,1:T(8,128)(2,1)} %convert_bitcast_fusion), calls=%async_computation.2 | async-start | bytes 8388608 | tf_op jit(solution)/shard_map/all_to_all | solution.py:87
  209.3 0.0 copy-done.5
  209.3 0.0 copy-done.8
  209.3 0.1 copy.34
  209.5 94.7 %all-to-all-done.2 = bf16[1,64,16,2048]{3,2,0,1:T(8,128)(2,1)} async-done(((bf16[1,64,16,2048]{3,2,0,1:T(8,128)(2,1)}), bf16[1,64,16,2048]{3,2,0,1:T(8,128)(2,1)}, u32[]{:S(2)}, u32[]{:S(2)}) %all-to-all-start.2) | async-done | bytes 4194336 | tf_op jit(solution)/shard_map/all_to_all | solution.py:87
  304.2 8.0 %gather_fusion.1 = bf16[512,2048]{1,0:T(8,128)(2,1)} fusion(bf16[1024,2048]{1,0:T(8,128)(2,1)} %bitcast.21, s32[1024]{0:T(1024)S(1)} %pad_clamp_fusion), kind=kCustom, calls=%fused_computation.1 | custom fusion | bytes 4196352 | tf_op jit(solution)/shard_map/gather | solution.py:88
  312.1 5.4 %reshape.118 = f32[256,2,2048]{2,1,0:T(2,128)} reshape(bf16[512,2048]{1,0:T(8,128)(2,1)} %gather_fusion.1) | data formatting | bytes 6291456 | tf_op jit(solution)/shard_map/convert_element_type | solution.py:90
  317.6 0.0 copy-start.3
  317.6 9.0 %multiply_reduce_fusion = f32[256,2048]{1,0:T(8,128)S(1)} fusion(f32[256,2,2048]{2,1,0:T(2,128)} %reshape.118, f32[256,2]{1,0:T(8,128)S(1)} %copy.34), kind=kLoop, calls=%fused_computation.7 | loop fusion | flops 1572864 | bytes 6293504 | tf_op jit(solution)/shard_map/reduce_sum | solution.py:90
  326.5 0.0 copy-done.3
  326.5 1.3 fusion.8
  (17 shorter events, 0.1 us)
Async XLA Ops:
  6.5 185.3 %copy-start = (bf16[1,512,2048]{2,1,0:T(8,128)(2,1)S(1)}, bf16[1,512,2048]{2,1,0:T(8,128)(2,1)}, u32[]{:S(2)}) copy-start(bf16[1,512,2048]{2,1,0:T(8,128)(2,1)} %param.27) | copy-start | bytes 6291460
  6.5 6.6 %copy-start.4 = (s32[256,2]{0,1:T(2,128)S(1)}, s32[256,2]{0,1:T(2,128)}, u32[]{:S(2)}) copy-start(s32[256,2]{0,1:T(2,128)} %param.22) | copy-start | bytes 6148
  6.5 8.5 %copy-start.6 = (bf16[3,256]{1,0:T(4,128)(2,1)S(1)}, bf16[3,256]{1,0:T(4,128)(2,1)}, u32[]{:S(2)}) copy-start(bf16[3,256]{1,0:T(4,128)(2,1)} %param.18) | copy-start | bytes 4612
  6.5 8.7 %copy-start.10 = (bf16[256]{0:T(256)(128)(2,1)S(1)}, bf16[256]{0:T(256)(128)(2,1)}, u32[]{:S(2)}) copy-start(bf16[256]{0:T(256)(128)(2,1)} %param.19) | copy-start | bytes 1540
  6.5 16.7 %copy-start.7 = (bf16[2048]{0:T(1024)(128)(2,1)S(1)}, bf16[2048]{0:T(1024)(128)(2,1)}, u32[]{:S(2)}) copy-start(bf16[2048]{0:T(1024)(128)(2,1)} %param.21) | copy-start | bytes 12292
  6.5 62.7 %all-gather.3.cloned.1.call-start = ((), (), s32[]{:S(2)}) async-start(), calls=%async_computation.3 | async-start | bytes 5242880 | tf_op jit(solution)/shard_map/all_gather | solution.py:49
  8.6 14.9 %collective-permute-start = (f32[2,256]{1,0:T(2,128)S(1)}, f32[2,256]{1,0:T(2,128)S(1)}, u32[]{:S(2)}, u32[]{:S(2)}) collective-permute-start(f32[2,256]{1,0:T(2,128)S(1)} %slice.37), channel_id=1, source_target_pairs={{0,4},{4,8},{8,12},{12,16},{16,20},{20,24},{24,28},{28,32},{32,36}... | collective-permute-start | bytes 6152 | tf_op jit(solution)/shard_map/ppermute | solution.py:12
  25.8 18.9 %all-to-all-start = ((bf16[4,256,256]{2,1,0:T(8,128)(2,1)}), bf16[4,256,256]{2,1,0:T(8,128)(2,1)S(1)}, u32[]{:S(2)}, u32[]{:S(2)}) async-start(bf16[4,256,256]{2,1,0:T(8,128)(2,1)} %bitcast.66), calls=%async_computation | async-start | bytes 1048576 | tf_op jit(solution)/shard_map/all_to_all | solution.py:47
  73.1 1.0 copy-start.2
  80.5 107.6 %copy-start.9 = (bf16[1,2048,512]{2,1,0:T(8,128)(2,1)S(1)}, bf16[1,2048,512]{2,1,0:T(8,128)(2,1)}, u32[]{:S(2)}) copy-start(bf16[1,2048,512]{2,1,0:T(8,128)(2,1)} %param.25) | copy-start | bytes 6291460
  186.1 2.0 copy-start.1
  201.8 7.5 %copy-start.5 = (f32[256,2]{0,1:T(2,128)S(1)}, f32[256,2]{0,1:T(2,128)}, u32[]{:S(2)}) copy-start(f32[256,2]{0,1:T(2,128)} %param.24) | copy-start | bytes 6148
  201.8 7.5 %copy-start.8 = (f32[256]{0:T(256)S(1)}, f32[256]{0:T(256)}, u32[]{:S(2)}) copy-start(f32[256]{0:T(256)} %param.23) | copy-start | bytes 3076
  201.8 102.4 %all-to-all-start.2 = ((bf16[1,64,16,2048]{3,2,0,1:T(8,128)(2,1)}), bf16[1,64,16,2048]{3,2,0,1:T(8,128)(2,1)}, u32[]{:S(2)}, u32[]{:S(2)}) async-start(bf16[1,64,16,2048]{3,2,0,1:T(8,128)(2,1)} %convert_bitcast_fusion), calls=%async_computation.2 | async-start | bytes 8388608 | tf_op jit(solution)/shard_map/all_to_all | solution.py:87
  317.6 9.0 %copy-start.3 = (bf16[256,2048]{1,0:T(8,128)(2,1)S(1)}, bf16[256,2048]{1,0:T(8,128)(2,1)}, u32[]{:S(2)}) copy-start(bf16[256,2048]{1,0:T(8,128)(2,1)} %copy-done.2) | copy-start | bytes 3145732
Sparse Core Ops, SparseCore 0:
  9.2 60.0 all-gather.2
where the time goes:
time: 336 us; the launch traced here: 335 us
  waiting for transfers between devices  128 us (38%)
  blocking collectives  114 us (34%)
  local copies, waits for them, and re-layouts  28.5 us (8%)
  other arithmetic  18.2 us (5%)
  matrix products  17.6 us (5%)
  starting transfers between devices  15.5 us (5%)
  between operations  13.7 us (4%)
    all_to_all x1, blocking collectives, body(): lax.all_to_all(outgoing, 'sp', split_axis=1, concat_axis=1, tiled=True)  106 us
    all_to_all x1, waiting for transfers between devices, body(): lax.all_to_all(result, 'sp', split_axis=1, concat_axis=1, tiled=True)  94.7 us
    all_gather x1, waiting for transfers between devices, body(): lax.all_gather(out_weight, 'tp', axis=0, tiled=True)  19.3 us
    all_to_all x1, waiting for transfers between devices, body(): lax.all_to_all(mixed_out, 'tp', split_axis=0, concat_axis=1, tiled=True)  12.9 us
    dot_general x1, matrix products, body(): jnp.einsum('esrf,efd->esrd', hidden, expert_down, preferred_element_type=...  9.96 us
    reduce_sum x1, other arithmetic, body(): jnp.sum(slot_out.astype(jnp.float32) * weights[:, :, None], axis=1)  8.96 us
    all_gather x1, blocking collectives, body(): lax.all_gather(norm_gain, 'tp', axis=0, tiled=True)  7.97 us
    gather x1, local copies, waits for them, and re-layouts, body(): returned.reshape(-1, width)[position].reshape(tok_rows, top_count, width)  7.96 us
  transfers between devices with their start and end apart: 4, of which 3 were waited for; matrix products, arithmetic and copies ran while one was open for 4% of the time, Pallas kernels for 0%

commit v1 on v0

v1 whole, which is shorter than its diff:
```python
import jax
import jax.numpy as jnp
from jax import lax
from jax.experimental import pallas as pl
from jax.experimental.pallas import tpu as pltpu
from jax.sharding import PartitionSpec as P

EPSILON = 1e-06
NZ = 8
CAP = 16
NC = 4
MESH = pl.DeviceIdType.MESH
BF = jnp.bfloat16
F32 = jnp.float32


def moe_kernel(
    rows_ref,
    res_ref,
    meta_ref,
    wg_hbm,
    wu_hbm,
    wd_hbm,
    out_ref,
    metas,
    hop1,
    hop2,
    sel3,
    pack3,
    hop3,
    hop4,
    packed,
    arrived,
    results,
    ret0,
    ret1,
    big2,
    ret3,
    ret4,
    back4,
    send2,
    part2,
    send1,
    part1,
    hid,
    wg,
    wu,
    wd,
    wsem,
    msend,
    mrecv,
    zsend,
    zrecv,
    xsend,
    xrecv,
    ysend,
    yrecv,
    rsend,
    rrecv,
):
    tok, width = rows_ref.shape
    nj = lax.axis_size("sp") // NZ
    grp = nj * CAP
    half = grp // 2
    cw = width // NC
    sp = lax.axis_index("sp")
    tp = lax.axis_index("tp")
    z = sp // nj
    me_j = sp % nj
    step = (1, -1)
    near = (1, NZ - 1)
    far = (2, NZ - 2)
    both = [(n, d) for n in range(NC) for d in (0, 1)]

    def zval(offset):
        return lax.rem(z + offset + NZ, NZ)

    def zid(offset):
        return (zval(offset) * nj + me_j, tp)

    def jid(offset):
        return (z * nj + lax.rem(me_j + offset, nj), tp)

    def cols_of(n):
        return slice(n * cw, (n + 1) * cw)

    def slot_rows(b, j):
        return pl.ds(pl.multiple_of(b * grp + j * CAP, CAP), CAP)

    sent = []

    def remote(src, dst, send, recv, device):
        return pltpu.make_async_remote_copy(
            src_ref=src, dst_ref=dst, send_sem=send, recv_sem=recv, device_id=device, device_id_type=MESH
        )

    def start(copy):
        copy.start()
        sent.append(copy)

    wcopies = [
        pltpu.make_async_copy(wg_hbm.at[0], wg, wsem.at[0]),
        pltpu.make_async_copy(wu_hbm.at[0], wu, wsem.at[1]),
        pltpu.make_async_copy(wd_hbm.at[0], wd, wsem.at[2]),
    ]
    for copy in wcopies:
        copy.start()

    barrier = pltpu.get_barrier_semaphore()
    for offset in range(1, NZ):
        pl.semaphore_signal(barrier, inc=1, device_id=zid(offset), device_id_type=MESH)
    for offset in range(1, nj):
        pl.semaphore_signal(barrier, inc=1, device_id=jid(offset), device_id_type=MESH)
    pl.semaphore_wait(barrier, NZ + nj - 2)

    def mcopy(offset):
        return remote(meta_ref, metas.at[offset], msend.at[offset], mrecv.at[offset], zid(offset))

    for offset in range(1, NZ):
        start(mcopy(offset))

    def zcopy(hop, d, n):
        cols = cols_of(n)
        if hop == 0:
            src, dst = rows_ref.at[:, cols], hop1.at[d, :, cols]
        elif hop == 1:
            src, dst = hop1.at[d, :, cols], hop2.at[d, :, cols]
        elif hop == 2:
            src, dst = pack3.at[d, :, cols], hop3.at[d, :, cols]
        else:
            src, dst = hop3.at[d, grp : grp + half, cols], hop4.at[d * half : (d + 1) * half, cols]
        return remote(src, dst, zsend.at[hop, d, n], zrecv.at[hop, d, n], zid(step[d]))

    for n, d in both:
        start(zcopy(0, d, n))

    def meta_of(offset):
        return meta_ref if offset == 0 else metas.at[offset]

    def slots_of(rows, target, first):
        return (lax.broadcasted_iota(jnp.int32, (rows, tok), 0) + (first + target * grp)).astype(F32)

    def select(offset, target, rows, first=0):
        ref = meta_of(offset)
        slot = slots_of(rows, target, first)
        hit = jnp.where(slot == ref[0:1, :], 1.0, 0.0) + jnp.where(slot == ref[1:2, :], 1.0, 0.0)
        return hit.astype(BF)

    def spread(offset, target, rows, first=0):
        ref = meta_of(offset)
        slot = slots_of(rows, target, first)
        hit = jnp.where(slot == ref[0:1, :], ref[2:3, :], 0.0) + jnp.where(slot == ref[1:2, :], ref[3:4, :], 0.0)
        return hit.astype(BF)

    def combine(weights, rows):
        return lax.dot_general(weights, rows, (((0,), (0,)), ((), ())), preferred_element_type=F32)

    def xsource(b):
        if b < 5:
            return packed.at[b]
        if b < 7:
            return hop3.at[b - 5]
        return hop4

    def ytarget(b):
        if b == 0:
            return ret0
        if b < 3:
            return ret1.at[b - 1]
        if b < 5:
            return big2.at[b - 3]
        if b < 7:
            return ret3.at[b - 5]
        return ret4

    def xstart(b):
        src = xsource(b)
        for offset in range(1, nj):
            their = slot_rows(0, lax.rem(me_j + offset, nj))
            start(remote(src.at[their, :], arrived.at[slot_rows(b, me_j), :], xsend.at[b, offset], xrecv.at[b, offset], jid(offset)))
        arrived[slot_rows(b, me_j), :] = src[slot_rows(0, me_j), :]

    def xwait(b):
        for offset in range(1, nj):
            mine = slot_rows(b, me_j)
            remote(arrived.at[mine, :], arrived.at[mine, :], xsend.at[b, offset], xrecv.at[b, offset], jid(offset)).wait_recv()

    def ystart(b):
        dst = ytarget(b)
        for offset in range(1, nj):
            their = slot_rows(b, lax.rem(me_j + offset, nj))
            start(remote(results.at[their, :], dst.at[slot_rows(0, me_j), :], ysend.at[b, offset], yrecv.at[b, offset], jid(offset)))
        dst[slot_rows(0, me_j), :] = results[slot_rows(b, me_j), :]

    def ywait(b):
        dst = ytarget(b)
        for offset in range(1, nj):
            mine = slot_rows(0, me_j)
            remote(dst.at[mine, :], dst.at[mine, :], ysend.at[b, offset], yrecv.at[b, offset], jid(offset)).wait_recv()

    def pack(b, offset, block):
        chosen = select(offset, z, grp)
        for n in range(NC):
            cols = cols_of(n)
            packed[b, :, cols] = jnp.dot(chosen, block[:, cols], preferred_element_type=F32).astype(BF)

    fe = wg.shape[1]
    fw = fe // 2

    def experts(first, count):
        rows = count * grp
        base = first * grp

        def up(f, carry):
            cols = pl.ds(pl.multiple_of(f * fw, fw), fw)
            act = arrived[base : base + rows, :]
            g = jnp.dot(act, wg[:, cols], preferred_element_type=F32)
            u = jnp.dot(act, wu[:, cols], preferred_element_type=F32)
            hid[0:rows, cols] = (g * jax.nn.sigmoid(g) * u).astype(BF)
            return carry

        lax.fori_loop(0, 2, up, 0)

        def down(n, carry):
            cols = pl.ds(pl.multiple_of(n * cw, cw), cw)
            r = jnp.dot(hid[0:rows, :], wd[:, cols], preferred_element_type=F32)
            results[base : base + rows, cols] = r.astype(BF)
            return carry

        lax.fori_loop(0, NC, down, 0)

    pack(0, 0, rows_ref)
    xstart(0)
    for n, d in both:
        zcopy(0, d, n).wait_recv()
        start(zcopy(1, d, n))
    for offset in range(1, NZ):
        mcopy(offset).wait_recv()
    for d in (0, 1):
        pack(1 + d, near[d], hop1.at[d])
        xstart(1 + d)
    for copy in wcopies:
        copy.wait()
    xwait(0)
    experts(0, 1)
    ystart(0)
    for d in (0, 1):
        sel3[d, 0:grp, :] = select(far[d], zval(step[d]), grp)
        sel3[d, grp : grp + half, :] = select(far[d], zval(2 * step[d]), half, d * half)
    for n, d in both:
        zcopy(1, d, n).wait_recv()
        cols = cols_of(n)
        pack3[d, :, cols] = jnp.dot(sel3[d], hop2[d, :, cols], preferred_element_type=F32).astype(BF)
        start(zcopy(2, d, n))
    for d in (0, 1):
        pack(3 + d, far[d], hop2.at[d])
        xstart(3 + d)
    xwait(1)
    xwait(2)
    experts(1, 2)
    ystart(1)
    ystart(2)
    for n, d in both:
        zcopy(2, d, n).wait_recv()
        start(zcopy(3, d, n))
    xstart(5)
    xstart(6)
    xwait(3)
    xwait(4)
    experts(3, 2)
    ystart(3)
    ystart(4)
    for n, d in both:
        zcopy(3, d, n).wait_recv()
    xstart(7)
    xwait(5)
    xwait(6)
    experts(5, 2)
    ystart(5)
    ystart(6)
    xwait(7)
    experts(7, 1)
    ystart(7)

    def rcopy(kind, d, n):
        cols = cols_of(n)
        if kind == 0:
            src, dst = ret4.at[d * half : (d + 1) * half, cols], back4.at[d, :, cols]
        elif kind == 1:
            src, dst = ret3.at[d, :, cols], big2.at[d, grp : 2 * grp, cols]
        elif kind == 2:
            src, dst = back4.at[d, :, cols], big2.at[d, 2 * grp : 2 * grp + half, cols]
        elif kind == 3:
            src, dst = send2.at[d, :, cols], part2.at[d, :, cols]
        else:
            src, dst = send1.at[d, :, cols], part1.at[d, :, cols]
        return remote(src, dst, rsend.at[kind, d, n], rrecv.at[kind, d, n], zid(-step[d]))

    ywait(5)
    ywait(6)
    for n, d in both:
        start(rcopy(1, d, n))
    ywait(7)
    for n, d in both:
        start(rcopy(0, d, n))
    for b in range(5):
        ywait(b)
    for n, d in both:
        rcopy(0, d, n).wait_recv()
        start(rcopy(2, d, n))
    for n, d in both:
        rcopy(1, d, n).wait_recv()
        rcopy(2, d, n).wait_recv()
        cols = cols_of(n)
        total = combine(spread(far[d], z, grp), big2[d, 0:grp, cols])
        total = total + combine(spread(far[d], zval(step[d]), grp), big2[d, grp : 2 * grp, cols])
        total = total + combine(spread(far[d], zval(2 * step[d]), half, d * half), big2[d, 2 * grp : 2 * grp + half, cols])
        send2[d, :, cols] = total.astype(BF)
        start(rcopy(3, d, n))
    for n, d in both:
        rcopy(3, d, n).wait_recv()
        cols = cols_of(n)
        total = part2[d, :, cols].astype(F32) + combine(spread(near[d], z, grp), ret1[d, :, cols])
        send1[d, :, cols] = total.astype(BF)
        start(rcopy(4, d, n))
    own = spread(0, z, grp)
    for n in range(NC):
        rcopy(4, 0, n).wait_recv()
        rcopy(4, 1, n).wait_recv()
        cols = cols_of(n)
        total = res_ref[:, cols].astype(F32) + combine(own, ret0[:, cols])
        total = total + part1[0, :, cols].astype(F32) + part1[1, :, cols].astype(F32)
        out_ref[:, cols] = total.astype(BF)
    for copy in sent:
        copy.wait_send()


def moe(rows, res, meta, wg, wu, wd):
    tok, width = rows.shape
    fe = wg.shape[2]
    nj = lax.axis_size("sp") // NZ
    grp = nj * CAP
    half = grp // 2
    vmem = pl.BlockSpec(memory_space=pltpu.VMEM)
    hbm = pl.BlockSpec(memory_space=pl.ANY)
    dma = pltpu.SemaphoreType.DMA
    shapes = [
        ((NZ,) + meta.shape, F32),
        ((2, tok, width), BF),
        ((2, tok, width), BF),
        ((2, grp + half, tok), BF),
        ((2, grp + half, width), BF),
        ((2, grp + half, width), BF),
        ((grp, width), BF),
        ((5, grp, width), BF),
        ((8 * grp, width), BF),
        ((8 * grp, width), BF),
        ((grp, width), BF),
        ((2, grp, width), BF),
        ((2, 2 * grp + half, width), BF),
        ((2, grp, width), BF),
        ((grp, width), BF),
        ((2, half, width), BF),
        ((2, tok, width), BF),
        ((2, tok, width), BF),
        ((2, tok, width), BF),
        ((2, tok, width), BF),
        ((2 * grp, fe), BF),
        (wg.shape[1:], BF),
        (wu.shape[1:], BF),
        (wd.shape[1:], BF),
    ]
    sems = [(3,), (NZ,), (NZ,), (4, 2, NC), (4, 2, NC), (8, nj), (8, nj), (8, nj), (8, nj), (5, 2, NC), (5, 2, NC)]
    return pl.pallas_call(
        moe_kernel,
        out_shape=jax.ShapeDtypeStruct((tok, width), BF),
        in_specs=[vmem, vmem, vmem, hbm, hbm, hbm],
        out_specs=vmem,
        scratch_shapes=[pltpu.VMEM(s, t) for s, t in shapes] + [dma(s) for s in sems],
        compiler_params=pltpu.CompilerParams(
            collective_id=0, has_side_effects=True, vmem_limit_bytes=60 * 1024 * 1024
        ),
        name="moe",
    )(rows, res, meta, wg, wu, wd)


def from_behind(shard, axis, by):
    devices = lax.axis_size(axis)
    pairs = [(i, i + by) for i in range(devices) if 0 <= i + by < devices]
    return lax.ppermute(shard, axis, pairs)


def rms_norm(values, gain):
    floats = values.astype(F32)
    factor = lax.rsqrt(jnp.mean(floats * floats, axis=-1, keepdims=True) + EPSILON)
    return floats * factor * gain.astype(F32)


def slot_meta(expert_ids, group_prob, route_prob, experts_all):
    tok = expert_ids.shape[0]
    lane = jnp.arange(experts_all, dtype=jnp.int32)[None, :]
    hot0 = (expert_ids[:, 0:1] == lane).astype(BF)
    hot1 = (expert_ids[:, 1:2] == lane).astype(BF)
    row = jnp.arange(tok, dtype=jnp.int32)
    before = (row[:, None] > row[None, :]).astype(BF)
    ranks = jnp.dot(before, jnp.concatenate([hot0, hot1], axis=1), preferred_element_type=F32)
    count0 = jnp.sum(hot0.astype(F32), axis=0, keepdims=True)
    rank0 = jnp.sum(ranks[:, :experts_all] * hot0, axis=1)
    rank1 = jnp.sum((ranks[:, experts_all:] + count0) * hot1, axis=1)
    pos0 = expert_ids[:, 0].astype(F32) * CAP + rank0
    pos1 = expert_ids[:, 1].astype(F32) * CAP + rank1
    weights = group_prob[:, None] * route_prob / jnp.sum(route_prob, axis=1, keepdims=True)
    zero = jnp.zeros_like(pos0)
    return jnp.stack([pos0, pos1, weights[:, 0], weights[:, 1], zero, zero, zero, zero], axis=0)


def body(
    residual_in,
    gate_outer,
    gate_inner,
    conv_input,
    conv_taps,
    norm_gain,
    out_weight,
    moe_gain,
    expert_ids,
    group_prob,
    route_prob,
    expert_gate,
    expert_up,
    expert_down,
):
    seq_rows, channels = conv_input.shape
    taps_count = conv_taps.shape[0]
    inner = gate_inner.astype(F32) * conv_input.astype(F32)
    earlier = from_behind(inner[seq_rows - (taps_count - 1) :], "sp", 1)
    padded = jnp.concatenate([earlier, inner], axis=0)
    tap_f = conv_taps.astype(F32)
    filtered = jnp.zeros((seq_rows, channels), F32)
    for offset in range(taps_count):
        filtered = filtered + tap_f[offset][None, :] * padded[offset : offset + seq_rows]
    mixed_out = (gate_outer.astype(F32) * filtered).astype(BF)
    gathered = lax.all_to_all(mixed_out, "tp", split_axis=0, concat_axis=1, tiled=True)
    full_weight, full_gain = (
        lax.all_gather(out_weight, "tp", axis=0, tiled=True),
        lax.all_gather(norm_gain, "tp", axis=0, tiled=True),
    )
    normed = rms_norm(gathered, full_gain).astype(BF)
    projected = jnp.dot(normed, full_weight, preferred_element_type=F32)
    residual = (residual_in.astype(F32) + projected).astype(BF)
    routed_in = rms_norm(residual, moe_gain).astype(BF)
    experts_all = expert_gate.shape[0] * lax.axis_size("sp")
    meta = slot_meta(expert_ids, group_prob, route_prob, experts_all)
    return moe(routed_in, residual, meta, expert_gate, expert_up, expert_down)


def solution(mesh):
    in_specs = (
        P(("sp", "tp"), None),
        P("sp", "tp"),
        P("sp", "tp"),
        P("sp", "tp"),
        P(None, "tp"),
        P("tp"),
        P("tp", None),
        P(),
        P(("sp", "tp"), None),
        P(("sp", "tp")),
        P(("sp", "tp"), None),
        P("sp", None, None),
        P("sp", None, None),
        P("sp", None, None),
    )
    out_specs = P(("sp", "tp"), None)
    return jax.shard_map(body, mesh=mesh, in_specs=in_specs, out_specs=out_specs, check_vma=False)
```

time: 336 us -> 277 us (0.82)
  Pallas kernels: 0 us -> 199 us
  blocking collectives: 114 us -> 11.4 us
  waiting for transfers between devices: 128 us -> 32.3 us
  local copies, waits for them, and re-layouts: 28.5 us -> 3.3 us
  other arithmetic: 18.2 us -> 4.56 us
  matrix products: 17.6 us -> 4.1 us
  starting transfers between devices: 15.5 us -> 8.72 us
    pallas_call x0 -> x1, Pallas kernels: none -> 199 us  [moe(): pl.pallas_call(moe_kernel, out_shape=jax.ShapeDtypeStruct((tok, width), B...]
    all_to_all x1 -> x0, blocking collectives: 106 us -> none  [body(): lax.all_to_all(outgoing, 'sp', split_axis=1, concat_axis=1, tiled=True)]
    all_to_all x1 -> x0, waiting for transfers between devices: 94.7 us -> none  [body(): lax.all_to_all(result, 'sp', split_axis=1, concat_axis=1, tiled=True)]
    gather x2 -> x0, local copies, waits for them, and re-layouts: 14 us -> none  [the longest x1 7.96 us: body(): returned.reshape(-1, width)[position].reshape(tok_rows, top_count, width)]
    dot_general x3 -> x2, matrix products: 17.6 us -> 4.1 us  [the longest x1 3.9 us: body(): projected = jnp.dot(normed, full_weight, preferred_element_type=F32)]
    all_to_all x1, waiting for transfers between devices: 12.9 us -> 0.01 us  [body(): lax.all_to_all(mixed_out, 'tp', split_axis=0, concat_axis=1, tiled=True)]
    all_gather x1, waiting for transfers between devices: 19.3 us -> 31.3 us  [body(): lax.all_gather(out_weight, 'tp', axis=0, tiled=True)]
    reduce_sum x3, other arithmetic: 9.1 us -> 0.22 us  [the longest x1 0.11 us: slot_meta(): count0 = jnp.sum(hot0.astype(F32), axis=0, keepdims=True)]
  transfers between devices with their start and end apart: 4 -> 3, of which waited for: 3 -> 2; matrix products, arithmetic and copies ran while one was open for 4% -> 2% of each run, Pallas kernels for 0% -> 0%
where the time goes in v1:
time: 277 us
  Pallas kernels  199 us (72%)
  waiting for transfers between devices  32.3 us (12%)
  between operations  13.6 us (5%)
  blocking collectives  11.4 us (4%)
  starting transfers between devices  8.72 us (3%)
  other arithmetic  4.56 us (2%)
  matrix products  4.1 us (1%)
  local copies, waits for them, and re-layouts  3.3 us (1%)
    pallas_call x1, Pallas kernels, moe(): pl.pallas_call(moe_kernel, out_shape=jax.ShapeDtypeStruct((tok, width), B...  199 us
    all_gather x1, waiting for transfers between devices, body(): lax.all_gather(out_weight, 'tp', axis=0, tiled=True)  31.3 us
    all_gather x1, blocking collectives, body(): lax.all_gather(norm_gain, 'tp', axis=0, tiled=True)  11.4 us
  transfers between devices with their start and end apart: 3, of which 2 were waited for; matrix products, arithmetic and copies ran while one was open for 2% of the time, Pallas kernels for 0%

profile of v1, /device:TPU:1, one launch (start us, length us, event | category | flops | bytes accessed | tf_op | source)
XLA Modules:
  0.0 276.9 jit_solution(7108771229020239989)
XLA Ops:
  6.5 0.0 copy-start.2
  6.5 0.0 copy-start.3
  6.5 0.0 copy-start.6
  6.5 0.0 copy-start.4
  6.5 0.0 copy-start.1
  6.5 0.0 all-gather.3.cloned.1.call-start
  6.6 0.7 all-gather.3.cloned.1.call-update
  7.3 1.3 convert_multiply_fusion.3
  8.6 0.0 copy-start.7
  8.6 0.0 copy-start.5
  8.6 4.5 %collective-permute-start = (f32[2,256]{1,0:T(2,128)S(1)}, f32[2,256]{1,0:T(2,128)S(1)}, u32[]{:S(2)}, u32[]{:S(2)}) collective-permute-start(f32[2,256]{1,0:T(2,128)S(1)} %slice.51), channel_id=1, source_target_pairs={{0,4},{4,8},{8,12},{12,16},{16,20},{20,24},{24,28},{28,32},{32,36}... | collective-permute-start | bytes 6152 | tf_op jit(solution)/shard_map/ppermute | solution.py:390
  13.1 0.0 copy-done.2
  13.2 0.0 copy-done.3
  13.2 0.0 copy-done.6
  13.2 0.0 copy-done.4
  13.3 0.2 fusion.14
  13.5 0.4 collective-permute-done
  13.9 0.0 copy-done.1
  13.9 1.2 fusion.9
  15.1 4.2 %all-to-all-start = ((bf16[4,256,256]{2,1,0:T(8,128)(2,1)}), bf16[4,256,256]{2,1,0:T(8,128)(2,1)S(1)}, u32[]{:S(2)}, u32[]{:S(2)}) async-start(bf16[4,256,256]{2,1,0:T(8,128)(2,1)} %bitcast.3), calls=%async_computation | async-start | bytes 1048576 | tf_op jit(solution)/shard_map/all_to_all | solution.py:443
  19.2 0.1 convert_reduce_fusion
  19.3 0.0 copy-done.7
  19.4 11.4 %all-gather = bf16[4,1,256]{2,1,0:T(2,128)(2,1)S(1)} all-gather(bf16[1,1,256]{2,1,0:T(2,128)(2,1)S(1)} %reshape.73), channel_id=1, replica_groups=mesh['sp'=64,'tp'=4] {'tp'}, dimensions={0}, use_global_device_ids=true | all-gather | bytes 2560 | tf_op jit(solution)/shard_map/all_gather | solution.py:446
  30.7 0.0 copy-done.5
  30.8 0.1 fusion.17
  30.9 0.6 stack.9.meta_ref
  31.5 0.0 all-to-all-done
  31.5 0.1 convert_bitcast_fusion
  31.6 0.3 copy.16
  31.9 0.2 fusion.10
  32.1 0.2 fusion.13
  32.3 31.3 %all-gather.3.cloned.1.call-done = bf16[1024,2048]{1,0:T(8,128)(2,1)} async-done(((bf16[256,2048]{1,0:T(8,128)(2,1)}), bf16[1024,2048]{1,0:T(8,128)(2,1)}) %all-gather.3.cloned.1.call-update) | async-done | bytes 4194320 | tf_op jit(solution)/shard_map/all_gather | solution.py:445
  63.6 3.9 %fusion.1 = (f32[256]{0:T(256)S(1)}, bf16[256,2048]{1,0:T(8,128)(2,1)S(1)}) fusion(bf16[256,1024]{0,1:T(8,128)(2,1)S(1)} %fusion.13, bf16[1024,2048]{1,0:T(8,128)(2,1)} %all-gather.3.cloned.1.call-done, bf16[256,2048]{1,0:T(8,128)(2,1)} %param.14), kind=kOutput, calls=%fused_computation.4 | convolution fusion | flops 1076887296 | bytes 6816768 | tf_op jit(solution)/shard_map/dot_general | solution.py:449
  67.5 0.0 copy-start
  67.5 1.3 fusion.3.rows_ref
  68.8 0.0 copy-done
  68.9 198.9 %moe.1 = bf16[256,2048]{1,0:T(8,128)(2,1)} custom-call(bf16[256,2048]{1,0:T(8,128)(2,1)} %fusion.3.rows_ref, bf16[256,2048]{1,0:T(8,128)(2,1)} %copy-done, f32[8,256]{1,0:T(8,128)} %stack.9.meta_ref, bf16[1,2048,512]{2,1,0:T(8,128)(2,1)} %wg_hbm.1, bf16[1,2048,512]{2,1,0:T(8,128)(2,1)} %wu_hbm.1, bf16[1,512,2048]{2,1,0:T(8,128)(2,1)} %wd_hbm.1), custom_call_target="tpu_custom_call" | custom-call | tf_op jit(solution)/shard_map/moe/pallas_call | solution.py:374
  267.8 2.3 copy.18
  (14 shorter events, 0.1 us)
Async XLA Ops:
  6.5 6.6 %copy-start.2 = (f32[256,2]{0,1:T(2,128)S(1)}, f32[256,2]{0,1:T(2,128)}, u32[]{:S(2)}) copy-start(f32[256,2]{0,1:T(2,128)} %param.24) | copy-start | bytes 6148
  6.5 6.6 %copy-start.3 = (s32[256,2]{0,1:T(2,128)S(1)}, s32[256,2]{0,1:T(2,128)}, u32[]{:S(2)}) copy-start(s32[256,2]{0,1:T(2,128)} %param.22) | copy-start | bytes 6148
  6.5 6.7 %copy-start.6 = (f32[256]{0:T(256)S(1)}, f32[256]{0:T(256)}, u32[]{:S(2)}) copy-start(f32[256]{0:T(256)} %param.23) | copy-start | bytes 3076
  6.5 6.7 %copy-start.4 = (bf16[3,256]{1,0:T(4,128)(2,1)S(1)}, bf16[3,256]{1,0:T(4,128)(2,1)}, u32[]{:S(2)}) copy-start(bf16[3,256]{1,0:T(4,128)(2,1)} %param.18) | copy-start | bytes 4612
  6.5 7.3 %copy-start.1 = (bf16[1024,256]{1,0:T(8,128)(2,1)S(1)}, bf16[1024,256]{1,0:T(8,128)(2,1)}, u32[]{:S(2)}) copy-start(bf16[1024,256]{1,0:T(8,128)(2,1)} %param.15) | copy-start | bytes 1572868
  6.5 57.1 %all-gather.3.cloned.1.call-start = ((), (), s32[]{:S(2)}) async-start(), calls=%async_computation.1 | async-start | bytes 5242880 | tf_op jit(solution)/shard_map/all_gather | solution.py:445
  8.6 10.7 %copy-start.7 = (bf16[256]{0:T(256)(128)(2,1)S(1)}, bf16[256]{0:T(256)(128)(2,1)}, u32[]{:S(2)}) copy-start(bf16[256]{0:T(256)(128)(2,1)} %param.19) | copy-start | bytes 1540
  8.6 22.1 %copy-start.5 = (bf16[2048]{0:T(1024)(128)(2,1)S(1)}, bf16[2048]{0:T(1024)(128)(2,1)}, u32[]{:S(2)}) copy-start(bf16[2048]{0:T(1024)(128)(2,1)} %param.21) | copy-start | bytes 12292
  8.6 5.2 %collective-permute-start = (f32[2,256]{1,0:T(2,128)S(1)}, f32[2,256]{1,0:T(2,128)S(1)}, u32[]{:S(2)}, u32[]{:S(2)}) collective-permute-start(f32[2,256]{1,0:T(2,128)S(1)} %slice.51), channel_id=1, source_target_pairs={{0,4},{4,8},{8,12},{12,16},{16,20},{20,24},{24,28},{28,32},{32,36}... | collective-permute-start | bytes 6152 | tf_op jit(solution)/shard_map/ppermute | solution.py:390
  15.1 16.4 %all-to-all-start = ((bf16[4,256,256]{2,1,0:T(8,128)(2,1)}), bf16[4,256,256]{2,1,0:T(8,128)(2,1)S(1)}, u32[]{:S(2)}, u32[]{:S(2)}) async-start(bf16[4,256,256]{2,1,0:T(8,128)(2,1)} %bitcast.3), calls=%async_computation | async-start | bytes 1048576 | tf_op jit(solution)/shard_map/all_to_all | solution.py:443
  67.5 1.3 copy-start
Sparse Core Ops, SparseCore 0:
  9.2 54.4 all-gather.2

commit v2 on v1

--- a/solution.py
+++ b/solution.py
@@ -26,18 +26,23 @@
     hop1,
     hop2,
     sel3,
+    sel4,
     pack3,
-    hop3,
-    hop4,
+    pack4,
+    gather3,
+    gather4,
+    pass4,
     packed,
     arrived,
     results,
     ret0,
     ret1,
-    big2,
+    ret2,
+    got3,
+    back4,
+    got4,
     ret3,
     ret4,
-    back4,
     send2,
     part2,
     send1,
@@ -55,14 +60,19 @@
     xrecv,
     ysend,
     yrecv,
+    gsend,
+    grecv,
+    bsend,
+    brecv,
     rsend,
     rrecv,
 ):
     tok, width = rows_ref.shape
     nj = lax.axis_size("sp") // NZ
     grp = nj * CAP
-    half = grp // 2
+    others = grp - CAP
     cw = width // NC
+    hw = cw // 2
     sp = lax.axis_index("sp")
     tp = lax.axis_index("tp")
     z = sp // nj
@@ -84,8 +94,17 @@
     def cols_of(n):
         return slice(n * cw, (n + 1) * cw)
 
+    def half_of(n):
+        return slice(n * hw, (n + 1) * hw)
+
+    def part_of(n, d):
+        return slice(n * cw + d * hw, n * cw + (d + 1) * hw)
+
     def slot_rows(b, j):
         return pl.ds(pl.multiple_of(b * grp + j * CAP, CAP), CAP)
+
+    def block_rows(b):
+        return slice(b * grp, (b + 1) * grp)
 
     sent = []
 
@@ -97,6 +116,9 @@
     def start(copy):
         copy.start()
         sent.append(copy)
+
+    def wait_bytes(ref, sem):
+        pltpu.make_async_copy(ref, ref, sem).wait()
 
     wcopies = [
         pltpu.make_async_copy(wg_hbm.at[0], wg, wsem.at[0]),
@@ -126,9 +148,11 @@
         elif hop == 1:
             src, dst = hop1.at[d, :, cols], hop2.at[d, :, cols]
         elif hop == 2:
-            src, dst = pack3.at[d, :, cols], hop3.at[d, :, cols]
+            src, dst = gather3.at[d, :, cols], arrived.at[block_rows(5 + d), cols]
+        elif hop == 3:
+            src, dst = gather4.at[d, :, half_of(n)], pass4.at[d, :, half_of(n)]
         else:
-            src, dst = hop3.at[d, grp : grp + half, cols], hop4.at[d * half : (d + 1) * half, cols]
+            src, dst = pass4.at[d, :, half_of(n)], arrived.at[block_rows(7), part_of(n, d)]
         return remote(src, dst, zsend.at[hop, d, n], zrecv.at[hop, d, n], zid(step[d]))
 
     for n, d in both:
@@ -137,69 +161,63 @@
     def meta_of(offset):
         return meta_ref if offset == 0 else metas.at[offset]
 
-    def slots_of(rows, target, first):
-        return (lax.broadcasted_iota(jnp.int32, (rows, tok), 0) + (first + target * grp)).astype(F32)
-
-    def select(offset, target, rows, first=0):
+    def slots_of(target):
+        return (lax.broadcasted_iota(jnp.int32, (grp, tok), 0) + target * grp).astype(F32)
+
+    def select(offset, target):
         ref = meta_of(offset)
-        slot = slots_of(rows, target, first)
+        slot = slots_of(target)
         hit = jnp.where(slot == ref[0:1, :], 1.0, 0.0) + jnp.where(slot == ref[1:2, :], 1.0, 0.0)
         return hit.astype(BF)
 
-    def spread(offset, target, rows, first=0):
+    def spread(offset, target):
         ref = meta_of(offset)
-        slot = slots_of(rows, target, first)
+        slot = slots_of(target)
         hit = jnp.where(slot == ref[0:1, :], ref[2:3, :], 0.0) + jnp.where(slot == ref[1:2, :], ref[3:4, :], 0.0)
         return hit.astype(BF)
 
     def combine(weights, rows):
         return lax.dot_general(weights, rows, (((0,), (0,)), ((), ())), preferred_element_type=F32)
 
-    def xsource(b):
-        if b < 5:
-            return packed.at[b]
-        if b < 7:
-            return hop3.at[b - 5]
-        return hop4
-
     def ytarget(b):
-        if b == 0:
-            return ret0
-        if b < 3:
-            return ret1.at[b - 1]
-        if b < 5:
-            return big2.at[b - 3]
-        if b < 7:
-            return ret3.at[b - 5]
-        return ret4
+        return ret0 if b == 0 else ret1.at[b - 1] if b < 3 else ret2.at[b - 3]
 
     def xstart(b):
-        src = xsource(b)
         for offset in range(1, nj):
             their = slot_rows(0, lax.rem(me_j + offset, nj))
-            start(remote(src.at[their, :], arrived.at[slot_rows(b, me_j), :], xsend.at[b, offset], xrecv.at[b, offset], jid(offset)))
-        arrived[slot_rows(b, me_j), :] = src[slot_rows(0, me_j), :]
+            start_only(remote(packed.at[b, their, :], arrived.at[slot_rows(b, me_j), :], xsend.at[b], xrecv.at[b], jid(offset)))
+        arrived[slot_rows(b, me_j), :] = packed[b, slot_rows(0, me_j), :]
+        pending.append((packed.at[b, 0:others, :], xsend.at[b]))
+
+    pending = []
+
+    def start_only(copy):
+        copy.start()
 
     def xwait(b):
-        for offset in range(1, nj):
-            mine = slot_rows(b, me_j)
-            remote(arrived.at[mine, :], arrived.at[mine, :], xsend.at[b, offset], xrecv.at[b, offset], jid(offset)).wait_recv()
+        wait_bytes(arrived.at[b * grp : b * grp + others, :], xrecv.at[b])
 
     def ystart(b):
         dst = ytarget(b)
         for offset in range(1, nj):
             their = slot_rows(b, lax.rem(me_j + offset, nj))
-            start(remote(results.at[their, :], dst.at[slot_rows(0, me_j), :], ysend.at[b, offset], yrecv.at[b, offset], jid(offset)))
+            start_only(remote(results.at[their, :], dst.at[slot_rows(0, me_j), :], ysend.at[b], yrecv.at[b], jid(offset)))
         dst[slot_rows(0, me_j), :] = results[slot_rows(b, me_j), :]
+        pending.append((dst.at[0:others, :], ysend.at[b]))
 
     def ywait(b):
-        dst = ytarget(b)
+        wait_bytes(ytarget(b).at[0:others, :], yrecv.at[b])
+
+    def exchange(src, dst, d, cols, ssem, rsem):
+        mine = slot_rows(0, me_j)
         for offset in range(1, nj):
-            mine = slot_rows(0, me_j)
-            remote(dst.at[mine, :], dst.at[mine, :], ysend.at[b, offset], yrecv.at[b, offset], jid(offset)).wait_recv()
+            their = slot_rows(0, lax.rem(me_j + offset, nj))
+            start_only(remote(src.at[d, their, cols], dst.at[d, mine, cols], ssem, rsem, jid(offset)))
+        dst[d, mine, cols] = src[d, mine, cols]
+        pending.append((src.at[d, 0:others, cols], ssem))
 
     def pack(b, offset, block):
-        chosen = select(offset, z, grp)
+        chosen = select(offset, z)
         for n in range(NC):
             cols = cols_of(n)
             packed[b, :, cols] = jnp.dot(chosen, block[:, cols], preferred_element_type=F32).astype(BF)
@@ -229,110 +247,159 @@
 
         lax.fori_loop(0, NC, down, 0)
 
-    pack(0, 0, rows_ref)
-    xstart(0)
-    for n, d in both:
-        zcopy(0, d, n).wait_recv()
+    with jax.named_scope("own"):
+        pack(0, 0, rows_ref)
+        xstart(0)
+    for n, d in both:
+        with jax.named_scope(f"hop1_{n}{d}"):
+            zcopy(0, d, n).wait_recv()
         start(zcopy(1, d, n))
-    for offset in range(1, NZ):
-        mcopy(offset).wait_recv()
-    for d in (0, 1):
-        pack(1 + d, near[d], hop1.at[d])
-        xstart(1 + d)
+    with jax.named_scope("metas"):
+        for offset in range(1, NZ):
+            mcopy(offset).wait_recv()
+    with jax.named_scope("pack1"):
+        for d in (0, 1):
+            pack(1 + d, near[d], hop1.at[d])
+            xstart(1 + d)
     for copy in wcopies:
         copy.wait()
+    for d in (0, 1):
+        sel3[d] = select(far[d], zval(step[d]))
+        sel4[d] = select(far[d], zval(2 * step[d]))
     xwait(0)
-    experts(0, 1)
-    ystart(0)
-    for d in (0, 1):
-        sel3[d, 0:grp, :] = select(far[d], zval(step[d]), grp)
-        sel3[d, grp : grp + half, :] = select(far[d], zval(2 * step[d]), half, d * half)
-    for n, d in both:
-        zcopy(1, d, n).wait_recv()
-        cols = cols_of(n)
-        pack3[d, :, cols] = jnp.dot(sel3[d], hop2[d, :, cols], preferred_element_type=F32).astype(BF)
-        start(zcopy(2, d, n))
-    for d in (0, 1):
-        pack(3 + d, far[d], hop2.at[d])
-        xstart(3 + d)
+    with jax.named_scope("exp0"):
+        experts(0, 1)
+
+    def hop3_out(n):
+        for d in (0, 1):
+            with jax.named_scope(f"ex{n}{d}"):
+                wait_bytes(gather3.at[d, 0:others, cols_of(n)], grecv.at[0, d, n])
+                wait_bytes(gather4.at[d, 0:others, half_of(n)], grecv.at[1, d, n])
+            start(zcopy(3, d, n))
+            start(zcopy(2, d, n))
+
+    for n in range(NC):
+        for d in (0, 1):
+            with jax.named_scope(f"hop2_{n}{d}"):
+                zcopy(1, d, n).wait_recv()
+            part = hop2[d, :, cols_of(n)]
+            pack3[d, :, cols_of(n)] = jnp.dot(sel3[d], part, preferred_element_type=F32).astype(BF)
+            part = hop2[d, :, part_of(n, d)]
+            pack4[d, :, half_of(n)] = jnp.dot(sel4[d], part, preferred_element_type=F32).astype(BF)
+            exchange(pack4, gather4, d, half_of(n), gsend.at[1, d, n], grecv.at[1, d, n])
+            exchange(pack3, gather3, d, cols_of(n), gsend.at[0, d, n], grecv.at[0, d, n])
+        if n > 0:
+            hop3_out(n - 1)
+    with jax.named_scope("pack2"):
+        for d in (0, 1):
+            pack(3 + d, far[d], hop2.at[d])
+            xstart(3 + d)
+    hop3_out(NC - 1)
     xwait(1)
     xwait(2)
-    experts(1, 2)
-    ystart(1)
-    ystart(2)
-    for n, d in both:
-        zcopy(2, d, n).wait_recv()
-        start(zcopy(3, d, n))
-    xstart(5)
-    xstart(6)
-    xwait(3)
-    xwait(4)
-    experts(3, 2)
-    ystart(3)
-    ystart(4)
-    for n, d in both:
-        zcopy(3, d, n).wait_recv()
-    xstart(7)
-    xwait(5)
-    xwait(6)
-    experts(5, 2)
-    ystart(5)
-    ystart(6)
-    xwait(7)
-    experts(7, 1)
-    ystart(7)
+    with jax.named_scope("exp12"):
+        experts(1, 2)
 
     def rcopy(kind, d, n):
         cols = cols_of(n)
         if kind == 0:
-            src, dst = ret4.at[d * half : (d + 1) * half, cols], back4.at[d, :, cols]
+            src, dst = results.at[block_rows(7), part_of(n, d)], back4.at[d, :, half_of(n)]
         elif kind == 1:
-            src, dst = ret3.at[d, :, cols], big2.at[d, grp : 2 * grp, cols]
+            src, dst = results.at[block_rows(5 + d), cols], got3.at[d, :, cols]
         elif kind == 2:
-            src, dst = back4.at[d, :, cols], big2.at[d, 2 * grp : 2 * grp + half, cols]
+            src, dst = back4.at[d, :, half_of(n)], got4.at[d, :, half_of(n)]
         elif kind == 3:
             src, dst = send2.at[d, :, cols], part2.at[d, :, cols]
         else:
             src, dst = send1.at[d, :, cols], part1.at[d, :, cols]
         return remote(src, dst, rsend.at[kind, d, n], rrecv.at[kind, d, n], zid(-step[d]))
 
-    ywait(5)
-    ywait(6)
+    for n, d in both:
+        with jax.named_scope(f"hop3_{n}{d}"):
+            zcopy(3, d, n).wait_recv()
+        start(zcopy(4, d, n))
+    xwait(3)
+    xwait(4)
+    with jax.named_scope("exp34"):
+        experts(3, 2)
+    ystart(3)
+    ystart(4)
+    with jax.named_scope("hop3w"):
+        for n, d in both:
+            zcopy(2, d, n).wait_recv()
+    with jax.named_scope("exp56"):
+        experts(5, 2)
     for n, d in both:
         start(rcopy(1, d, n))
-    ywait(7)
+    with jax.named_scope("hop4w"):
+        for n, d in both:
+            zcopy(4, d, n).wait_recv()
+    with jax.named_scope("exp7"):
+        experts(7, 1)
     for n, d in both:
         start(rcopy(0, d, n))
-    for b in range(5):
-        ywait(b)
-    for n, d in both:
-        rcopy(0, d, n).wait_recv()
+    for n, d in both:
+        with jax.named_scope(f"r3_{n}{d}"):
+            rcopy(1, d, n).wait_recv()
+        exchange(got3, ret3, d, cols_of(n), bsend.at[0, d, n], brecv.at[0, d, n])
+    for n, d in both:
+        with jax.named_scope(f"r4_{n}{d}"):
+            rcopy(0, d, n).wait_recv()
         start(rcopy(2, d, n))
-    for n, d in both:
-        rcopy(1, d, n).wait_recv()
-        rcopy(2, d, n).wait_recv()
+    ywait(3)
+    ywait(4)
+
+    def sums2_out(n):
+        for d in (0, 1):
+            with jax.named_scope(f"ex{n}{d}"):
+                wait_bytes(ret3.at[d, 0:others, cols_of(n)], brecv.at[0, d, n])
+                wait_bytes(ret4.at[d, 0:others, half_of(n)], brecv.at[1, d, n])
+            total = combine(spread(far[d], z), ret2[d, :, cols_of(n)])
+            total = total + combine(spread(far[d], zval(step[d])), ret3[d, :, cols_of(n)])
+            last = combine(spread(far[d], zval(2 * step[d])), ret4[d, :, half_of(n)])
+            lo, hi = total[:, :hw], total[:, hw:]
+            if d == 0:
+                lo = lo + last
+            else:
+                hi = hi + last
+            send2[d, :, part_of(n, 0)] = lo.astype(BF)
+            send2[d, :, part_of(n, 1)] = hi.astype(BF)
+            start(rcopy(3, d, n))
+
+    for n in range(NC):
+        for d in (0, 1):
+            with jax.named_scope(f"r3b_{n}{d}"):
+                rcopy(2, d, n).wait_recv()
+            exchange(got4, ret4, d, half_of(n), bsend.at[1, d, n], brecv.at[1, d, n])
+        if n > 0:
+            sums2_out(n - 1)
+    sums2_out(NC - 1)
+    ystart(1)
+    ystart(2)
+    ystart(0)
+    ywait(1)
+    ywait(2)
+    for n, d in both:
+        with jax.named_scope(f"r2_{n}{d}"):
+            rcopy(3, d, n).wait_recv()
         cols = cols_of(n)
-        total = combine(spread(far[d], z, grp), big2[d, 0:grp, cols])
-        total = total + combine(spread(far[d], zval(step[d]), grp), big2[d, grp : 2 * grp, cols])
-        total = total + combine(spread(far[d], zval(2 * step[d]), half, d * half), big2[d, 2 * grp : 2 * grp + half, cols])
-        send2[d, :, cols] = total.astype(BF)
-        start(rcopy(3, d, n))
-    for n, d in both:
-        rcopy(3, d, n).wait_recv()
-        cols = cols_of(n)
-        total = part2[d, :, cols].astype(F32) + combine(spread(near[d], z, grp), ret1[d, :, cols])
+        total = part2[d, :, cols].astype(F32) + combine(spread(near[d], z), ret1[d, :, cols])
         send1[d, :, cols] = total.astype(BF)
         start(rcopy(4, d, n))
-    own = spread(0, z, grp)
+    ywait(0)
+    own = spread(0, z)
     for n in range(NC):
-        rcopy(4, 0, n).wait_recv()
-        rcopy(4, 1, n).wait_recv()
+        with jax.named_scope(f"r1_{n}"):
+            rcopy(4, 0, n).wait_recv()
+            rcopy(4, 1, n).wait_recv()
         cols = cols_of(n)
         total = res_ref[:, cols].astype(F32) + combine(own, ret0[:, cols])
         total = total + part1[0, :, cols].astype(F32) + part1[1, :, cols].astype(F32)
         out_ref[:, cols] = total.astype(BF)
     for copy in sent:
         copy.wait_send()
+    for ref, sem in pending:
+        wait_bytes(ref, sem)
 
 
 def moe(rows, res, meta, wg, wu, wd):
@@ -340,7 +407,6 @@
     fe = wg.shape[2]
     nj = lax.axis_size("sp") // NZ
     grp = nj * CAP
-    half = grp // 2
     vmem = pl.BlockSpec(memory_space=pltpu.VMEM)
     hbm = pl.BlockSpec(memory_space=pl.ANY)
     dma = pltpu.SemaphoreType.DMA
@@ -348,19 +414,24 @@
         ((NZ,) + meta.shape, F32),
         ((2, tok, width), BF),
         ((2, tok, width), BF),
-        ((2, grp + half, tok), BF),
-        ((2, grp + half, width), BF),
-        ((2, grp + half, width), BF),
-        ((grp, width), BF),
+        ((2, grp, tok), BF),
+        ((2, grp, tok), BF),
+        ((2, grp, width), BF),
+        ((2, grp, width // 2), BF),
+        ((2, grp, width), BF),
+        ((2, grp, width // 2), BF),
+        ((2, grp, width // 2), BF),
         ((5, grp, width), BF),
         ((8 * grp, width), BF),
         ((8 * grp, width), BF),
         ((grp, width), BF),
         ((2, grp, width), BF),
-        ((2, 2 * grp + half, width), BF),
         ((2, grp, width), BF),
-        ((grp, width), BF),
-        ((2, half, width), BF),
+        ((2, grp, width), BF),
+        ((2, grp, width // 2), BF),
+        ((2, grp, width // 2), BF),
+        ((2, grp, width), BF),
+        ((2, grp, width // 2), BF),
         ((2, tok, width), BF),
         ((2, tok, width), BF),
         ((2, tok, width), BF),
@@ -370,7 +441,8 @@
         (wu.shape[1:], BF),
         (wd.shape[1:], BF),
     ]
-    sems = [(3,), (NZ,), (NZ,), (4, 2, NC), (4, 2, NC), (8, nj), (8, nj), (8, nj), (8, nj), (5, 2, NC), (5, 2, NC)]
+    sems = [(3,), (NZ,), (NZ,), (5, 2, NC), (5, 2, NC), (5,), (5,), (5,), (5,)]
+    sems += [(2, 2, NC), (2, 2, NC), (2, 2, NC), (2, 2, NC), (5, 2, NC), (5, 2, NC)]
     return pl.pallas_call(
         moe_kernel,
         out_shape=jax.ShapeDtypeStruct((tok, width), BF),

time: 277 us -> 238 us (0.86)
  Pallas kernels: 199 us -> 159 us
    pallas_call x1, Pallas kernels: 199 us -> 159 us  [moe(): pl.pallas_call(moe_kernel, out_shape=jax.ShapeDtypeStruct((tok, width), B...]
where the time goes in v2:
time: 238 us; the launch traced here: 237 us
  Pallas kernels  159 us (67%)
  waiting for transfers between devices  32.3 us (14%)
  between operations  13.6 us (6%)
  blocking collectives  11.4 us (5%)
  starting transfers between devices  8.72 us (4%)
  other arithmetic  4.56 us (2%)
  matrix products  4.1 us (2%)
  local copies, waits for them, and re-layouts  3.3 us (1%)
    pallas_call x1, Pallas kernels, moe(): pl.pallas_call(moe_kernel, out_shape=jax.ShapeDtypeStruct((tok, width), B...  159 us
    all_gather x1, waiting for transfers between devices, body(): lax.all_gather(out_weight, 'tp', axis=0, tiled=True)  31.3 us
    all_gather x1, blocking collectives, body(): lax.all_gather(norm_gain, 'tp', axis=0, tiled=True)  11.4 us
  transfers between devices with their start and end apart: 3, of which 2 were waited for; matrix products, arithmetic and copies ran while one was open for 2% of the time, Pallas kernels for 0%

profile of v2, /device:TPU:1, one launch (start us, length us, event | category | flops | bytes accessed | tf_op | source)
XLA Modules:
  0.0 237.3 jit_solution(3290345592574833312)
XLA Ops:
  6.5 0.0 copy-start.2
  6.5 0.0 copy-start.3
  6.5 0.0 copy-start.6
  6.5 0.0 copy-start.4
  6.5 0.0 copy-start.1
  6.5 0.0 all-gather.3.cloned.1.call-start
  6.6 0.7 all-gather.3.cloned.1.call-update
  7.3 1.3 convert_multiply_fusion.3
  8.6 0.0 copy-start.7
  8.6 0.0 copy-start.5
  8.6 4.5 %collective-permute-start = (f32[2,256]{1,0:T(2,128)S(1)}, f32[2,256]{1,0:T(2,128)S(1)}, u32[]{:S(2)}, u32[]{:S(2)}) collective-permute-start(f32[2,256]{1,0:T(2,128)S(1)} %slice.51), channel_id=1, source_target_pairs={{0,4},{4,8},{8,12},{12,16},{16,20},{20,24},{24,28},{28,32},{32,36}... | collective-permute-start | bytes 6152 | tf_op jit(solution)/shard_map/ppermute | solution.py:462
  13.1 0.0 copy-done.2
  13.2 0.0 copy-done.3
  13.2 0.0 copy-done.6
  13.2 0.0 copy-done.4
  13.3 0.2 fusion.14
  13.5 0.4 collective-permute-done
  13.9 0.0 copy-done.1
  13.9 1.2 fusion.9
  15.1 4.2 %all-to-all-start = ((bf16[4,256,256]{2,1,0:T(8,128)(2,1)}), bf16[4,256,256]{2,1,0:T(8,128)(2,1)S(1)}, u32[]{:S(2)}, u32[]{:S(2)}) async-start(bf16[4,256,256]{2,1,0:T(8,128)(2,1)} %bitcast.3), calls=%async_computation | async-start | bytes 1048576 | tf_op jit(solution)/shard_map/all_to_all | solution.py:515
  19.2 0.1 convert_reduce_fusion
  19.3 0.0 copy-done.7
  19.4 11.4 %all-gather = bf16[4,1,256]{2,1,0:T(2,128)(2,1)S(1)} all-gather(bf16[1,1,256]{2,1,0:T(2,128)(2,1)S(1)} %reshape.73), channel_id=1, replica_groups=mesh['sp'=64,'tp'=4] {'tp'}, dimensions={0}, use_global_device_ids=true | all-gather | bytes 2560 | tf_op jit(solution)/shard_map/all_gather | solution.py:518
  30.7 0.0 copy-done.5
  30.8 0.1 fusion.17
  30.9 0.6 stack.9.meta_ref
  31.5 0.0 all-to-all-done
  31.5 0.1 convert_bitcast_fusion
  31.6 0.3 copy.16
  31.9 0.2 fusion.10
  32.1 0.2 fusion.13
  32.3 31.3 %all-gather.3.cloned.1.call-done = bf16[1024,2048]{1,0:T(8,128)(2,1)} async-done(((bf16[256,2048]{1,0:T(8,128)(2,1)}), bf16[1024,2048]{1,0:T(8,128)(2,1)}) %all-gather.3.cloned.1.call-update) | async-done | bytes 4194320 | tf_op jit(solution)/shard_map/all_gather | solution.py:517
  63.6 3.9 %fusion.1 = (f32[256]{0:T(256)S(1)}, bf16[256,2048]{1,0:T(8,128)(2,1)S(1)}) fusion(bf16[256,1024]{0,1:T(8,128)(2,1)S(1)} %fusion.13, bf16[1024,2048]{1,0:T(8,128)(2,1)} %all-gather.3.cloned.1.call-done, bf16[256,2048]{1,0:T(8,128)(2,1)} %param.14), kind=kOutput, calls=%fused_computation.4 | convolution fusion | flops 1076887296 | bytes 6816768 | tf_op jit(solution)/shard_map/dot_general | solution.py:521
  67.5 0.0 copy-start
  67.5 1.3 fusion.3.rows_ref
  68.8 0.0 copy-done
  68.9 159.3 %moe.1 = bf16[256,2048]{1,0:T(8,128)(2,1)} custom-call(bf16[256,2048]{1,0:T(8,128)(2,1)} %fusion.3.rows_ref, bf16[256,2048]{1,0:T(8,128)(2,1)} %copy-done, f32[8,256]{1,0:T(8,128)} %stack.9.meta_ref, bf16[1,2048,512]{2,1,0:T(8,128)(2,1)} %wg_hbm.1, bf16[1,2048,512]{2,1,0:T(8,128)(2,1)} %wu_hbm.1, bf16[1,512,2048]{2,1,0:T(8,128)(2,1)} %wd_hbm.1), custom_call_target="tpu_custom_call" | custom-call | tf_op jit(solution)/shard_map/moe/pallas_call | solution.py:446
  228.1 2.3 copy.18
  (14 shorter events, 0.1 us)
Async XLA Ops:
  6.5 6.6 %copy-start.2 = (f32[256,2]{0,1:T(2,128)S(1)}, f32[256,2]{0,1:T(2,128)}, u32[]{:S(2)}) copy-start(f32[256,2]{0,1:T(2,128)} %param.24) | copy-start | bytes 6148
  6.5 6.6 %copy-start.3 = (s32[256,2]{0,1:T(2,128)S(1)}, s32[256,2]{0,1:T(2,128)}, u32[]{:S(2)}) copy-start(s32[256,2]{0,1:T(2,128)} %param.22) | copy-start | bytes 6148
  6.5 6.7 %copy-start.6 = (f32[256]{0:T(256)S(1)}, f32[256]{0:T(256)}, u32[]{:S(2)}) copy-start(f32[256]{0:T(256)} %param.23) | copy-start | bytes 3076
  6.5 6.7 %copy-start.4 = (bf16[3,256]{1,0:T(4,128)(2,1)S(1)}, bf16[3,256]{1,0:T(4,128)(2,1)}, u32[]{:S(2)}) copy-start(bf16[3,256]{1,0:T(4,128)(2,1)} %param.18) | copy-start | bytes 4612
  6.5 7.3 %copy-start.1 = (bf16[1024,256]{1,0:T(8,128)(2,1)S(1)}, bf16[1024,256]{1,0:T(8,128)(2,1)}, u32[]{:S(2)}) copy-start(bf16[1024,256]{1,0:T(8,128)(2,1)} %param.15) | copy-start | bytes 1572868
  6.5 57.1 %all-gather.3.cloned.1.call-start = ((), (), s32[]{:S(2)}) async-start(), calls=%async_computation.1 | async-start | bytes 5242880 | tf_op jit(solution)/shard_map/all_gather | solution.py:517
  8.6 10.7 %copy-start.7 = (bf16[256]{0:T(256)(128)(2,1)S(1)}, bf16[256]{0:T(256)(128)(2,1)}, u32[]{:S(2)}) copy-start(bf16[256]{0:T(256)(128)(2,1)} %param.19) | copy-start | bytes 1540
  8.6 22.1 %copy-start.5 = (bf16[2048]{0:T(1024)(128)(2,1)S(1)}, bf16[2048]{0:T(1024)(128)(2,1)}, u32[]{:S(2)}) copy-start(bf16[2048]{0:T(1024)(128)(2,1)} %param.21) | copy-start | bytes 12292
  8.6 5.2 %collective-permute-start = (f32[2,256]{1,0:T(2,128)S(1)}, f32[2,256]{1,0:T(2,128)S(1)}, u32[]{:S(2)}, u32[]{:S(2)}) collective-permute-start(f32[2,256]{1,0:T(2,128)S(1)} %slice.51), channel_id=1, source_target_pairs={{0,4},{4,8},{8,12},{12,16},{16,20},{20,24},{24,28},{28,32},{32,36}... | collective-permute-start | bytes 6152 | tf_op jit(solution)/shard_map/ppermute | solution.py:462
  15.1 16.4 %all-to-all-start = ((bf16[4,256,256]{2,1,0:T(8,128)(2,1)}), bf16[4,256,256]{2,1,0:T(8,128)(2,1)S(1)}, u32[]{:S(2)}, u32[]{:S(2)}) async-start(bf16[4,256,256]{2,1,0:T(8,128)(2,1)} %bitcast.3), calls=%async_computation | async-start | bytes 1048576 | tf_op jit(solution)/shard_map/all_to_all | solution.py:515
  67.5 1.3 copy-start
Sparse Core Ops, SparseCore 0:
  9.2 54.4 all-gather.2

commit v3 on v2

--- a/solution.py
+++ b/solution.py
@@ -14,14 +14,38 @@
 F32 = jnp.float32
 
 
-def moe_kernel(
-    rows_ref,
-    res_ref,
-    meta_ref,
+def layer_kernel(
+    rin_hbm,
+    go_hbm,
+    gi_hbm,
+    ci_hbm,
+    ow_hbm,
     wg_hbm,
     wu_hbm,
     wd_hbm,
+    taps_ref,
+    gain_ref,
+    mgain_ref,
+    ids_ref,
+    group_ref,
+    route_ref,
     out_ref,
+    rin,
+    go,
+    gi,
+    ci,
+    ow,
+    halo,
+    inner,
+    mixed,
+    mixrel,
+    gainsrc,
+    gainrel,
+    normed,
+    wrel,
+    res_ref,
+    meta_ref,
+    act,
     metas,
     hop1,
     hop2,
@@ -51,7 +75,14 @@
     wg,
     wu,
     wd,
+    isem,
     wsem,
+    hsend,
+    hrecv,
+    tsend,
+    trecv,
+    asend,
+    arecv,
     msend,
     mrecv,
     zsend,
@@ -67,9 +98,12 @@
     rsend,
     rrecv,
 ):
-    tok, width = rows_ref.shape
-    nj = lax.axis_size("sp") // NZ
+    tok, width = res_ref.shape
+    nsp = lax.axis_size("sp")
+    ntp = lax.axis_size("tp")
+    nj = nsp // NZ
     grp = nj * CAP
+    seq, chan = mixed.shape
     others = grp - CAP
     cw = width // NC
     hw = cw // 2
@@ -91,6 +125,14 @@
     def jid(offset):
         return (z * nj + lax.rem(me_j + offset, nj), tp)
 
+    def tid(offset):
+        return (sp, lax.rem(tp + offset, ntp))
+
+    after = (lax.rem(sp + 1, nsp), tp)
+    before = (lax.rem(sp + nsp - 1, nsp), tp)
+    core = lax.rem(me_j, 2)
+    partner = (z * nj + me_j + 1 - 2 * core, tp)
+
     def cols_of(n):
         return slice(n * cw, (n + 1) * cw)
 
@@ -120,31 +162,35 @@
     def wait_bytes(ref, sem):
         pltpu.make_async_copy(ref, ref, sem).wait()
 
+    icopies = [
+        pltpu.make_async_copy(src, dst, isem.at[i])
+        for i, (src, dst) in enumerate(((ow_hbm, ow), (gi_hbm, gi), (ci_hbm, ci), (go_hbm, go), (rin_hbm, rin)))
+    ]
+    for copy in icopies:
+        copy.start()
     wcopies = [
         pltpu.make_async_copy(wg_hbm.at[0], wg, wsem.at[0]),
         pltpu.make_async_copy(wu_hbm.at[0], wu, wsem.at[1]),
         pltpu.make_async_copy(wd_hbm.at[0], wd, wsem.at[2]),
     ]
-    for copy in wcopies:
-        copy.start()
-
     barrier = pltpu.get_barrier_semaphore()
     for offset in range(1, NZ):
         pl.semaphore_signal(barrier, inc=1, device_id=zid(offset), device_id_type=MESH)
     for offset in range(1, nj):
         pl.semaphore_signal(barrier, inc=1, device_id=jid(offset), device_id_type=MESH)
-    pl.semaphore_wait(barrier, NZ + nj - 2)
+    for offset in range(1, ntp):
+        pl.semaphore_signal(barrier, inc=1, device_id=tid(offset), device_id_type=MESH)
+    for ident in (after, before):
+        pl.semaphore_signal(barrier, inc=1, device_id=ident, device_id_type=MESH)
+    pl.semaphore_wait(barrier, NZ + nj + ntp - 1)
 
     def mcopy(offset):
         return remote(meta_ref, metas.at[offset], msend.at[offset], mrecv.at[offset], zid(offset))
-
-    for offset in range(1, NZ):
-        start(mcopy(offset))
 
     def zcopy(hop, d, n):
         cols = cols_of(n)
         if hop == 0:
-            src, dst = rows_ref.at[:, cols], hop1.at[d, :, cols]
+            src, dst = res_ref.at[:, cols], hop1.at[d, :, cols]
         elif hop == 1:
             src, dst = hop1.at[d, :, cols], hop2.at[d, :, cols]
         elif hop == 2:
@@ -155,8 +201,140 @@
             src, dst = pass4.at[d, :, half_of(n)], arrived.at[block_rows(7), part_of(n, d)]
         return remote(src, dst, zsend.at[hop, d, n], zrecv.at[hop, d, n], zid(step[d]))
 
-    for n, d in both:
-        start(zcopy(0, d, n))
+    def own_cols(n):
+        return pl.ds(pl.multiple_of(n * cw + core * hw, hw), hw)
+
+    def quarter_cols(n, d):
+        return pl.ds(pl.multiple_of(n * cw + core * hw + d * (hw // 2), hw // 2), hw // 2)
+
+    def acopy(kind, n):
+        if kind == 0:
+            src, dst, device = ow.at[:, own_cols(n)], wrel.at[3, :, own_cols(n)], tid(1)
+        elif kind == 1:
+            src, dst, device = ow.at[:, own_cols(n)], wrel.at[1, :, own_cols(n)], tid(ntp - 1)
+        elif kind == 2:
+            cols = quarter_cols(n, 0)
+            src, dst, device = wrel.at[3, :, cols], wrel.at[2, :, cols], tid(1)
+        elif kind == 3:
+            cols = quarter_cols(n, 1)
+            src, dst, device = wrel.at[1, :, cols], wrel.at[2, :, cols], tid(ntp - 1)
+        else:
+            cols = own_cols(n)
+            block = (3, 1, 2)[kind - 4]
+            src, dst, device = wrel.at[block, :, cols], wrel.at[block, :, cols], partner
+        return remote(src, dst, asend.at[kind, n], arecv.at[kind, n], device)
+
+    def tcopy(offset):
+        rows = pl.ds(pl.multiple_of(lax.rem(tp + offset, ntp) * tok, tok), tok)
+        return remote(mixed.at[rows, :], mixrel.at[ntp - offset], tsend.at[0, offset], trecv.at[0, offset], tid(offset))
+
+    def gcopy(offset):
+        return remote(gainsrc, gainrel.at[ntp - offset], tsend.at[1, offset], trecv.at[1, offset], tid(offset))
+
+    def hcopy(i):
+        src = (gi, ci)[i]
+        return remote(src.at[seq - 16 : seq, :], halo.at[i], hsend.at[i], hrecv.at[i], after)
+
+    icopies[0].wait()
+    for kind in (0, 1):
+        start(acopy(kind, 0))
+    gainsrc[...] = jnp.broadcast_to(gain_ref[...].astype(F32), gainsrc.shape)
+    for offset in range(1, ntp):
+        start(gcopy(offset))
+    icopies[1].wait()
+    start(hcopy(0))
+    icopies[2].wait()
+    start(hcopy(1))
+    icopies[3].wait()
+    icopies[4].wait()
+    for copy in wcopies:
+        copy.start()
+    taps = taps_ref[...].astype(F32)
+    kw = taps_ref.shape[0]
+    with jax.named_scope("conv"):
+        inner[8 : 8 + seq, :] = gi[...].astype(F32) * ci[...].astype(F32)
+
+        def mix(first, rows):
+            filtered = taps[0:1, :] * inner[9 - kw + first : 9 - kw + first + rows, :]
+            for k in range(1, kw):
+                filtered = filtered + taps[k : k + 1, :] * inner[9 - kw + k + first : 9 - kw + k + first + rows, :]
+            mixed[first : first + rows, :] = (go[first : first + rows, :].astype(F32) * filtered).astype(BF)
+
+        mix(tok, seq - tok)
+    with jax.named_scope("halo"):
+        for i in (0, 1):
+            hcopy(i).wait_recv()
+    earlier = halo[0, 8:16, :].astype(F32) * halo[1, 8:16, :].astype(F32)
+    inner[0:8, :] = jnp.where(sp > 0, earlier, 0.0)
+    mix(0, tok)
+    for offset in range(1, ntp):
+        start(tcopy(offset))
+    for kind in (0, 1):
+        start(acopy(kind, 1))
+    mixrel[0] = mixed[pl.ds(pl.multiple_of(tp * tok, tok), tok), :]
+
+    with jax.named_scope("slots"):
+        expert = lax.broadcasted_iota(jnp.int32, (nsp, tok), 0)
+        hot = [jnp.where(expert == ids_ref[k : k + 1, :], 1.0, 0.0) for k in (0, 1)]
+        earlier_tok = lax.broadcasted_iota(jnp.int32, (tok, tok), 0) < lax.broadcasted_iota(jnp.int32, (tok, tok), 1)
+        upper = jnp.where(earlier_tok, 1.0, 0.0).astype(BF)
+        rank = [jnp.dot(h.astype(BF), upper, preferred_element_type=F32) for h in hot]
+        count = jnp.sum(hot[0], axis=1, keepdims=True)
+        slot = expert.astype(F32) * CAP
+        meta_ref[0:1, :] = jnp.sum((rank[0] + slot) * hot[0], axis=0, keepdims=True)
+        meta_ref[1:2, :] = jnp.sum((rank[1] + count + slot) * hot[1], axis=0, keepdims=True)
+        meta_ref[2:3, :] = group_ref[...] * route_ref[0:1, :] / (route_ref[0:1, :] + route_ref[1:2, :])
+        meta_ref[3:4, :] = group_ref[...] * route_ref[1:2, :] / (route_ref[0:1, :] + route_ref[1:2, :])
+        meta_ref[4:8, :] = jnp.zeros((4, tok), F32)
+    for offset in range(1, NZ):
+        start(mcopy(offset))
+
+    def pass_on(n):
+        acopy(0, n).wait_recv()
+        start(acopy(2, n))
+        start(acopy(4, n))
+        acopy(1, n).wait_recv()
+        start(acopy(3, n))
+        start(acopy(5, n))
+
+    with jax.named_scope("pass0"):
+        pass_on(0)
+    for kind in (0, 1):
+        start(acopy(kind, 2))
+    with jax.named_scope("rows"):
+        for offset in range(1, ntp):
+            tcopy(offset).wait_recv()
+            gcopy(offset).wait_recv()
+    gainrel[0] = gainsrc[...]
+    with jax.named_scope("norm"):
+        square = jnp.zeros((tok, 1), F32)
+        for o in range(ntp):
+            part = mixrel[o].astype(F32)
+            square = square + jnp.sum(part * part, axis=1, keepdims=True)
+        factor = lax.rsqrt(square / (chan * ntp) + EPSILON)
+        for o in range(ntp):
+            normed[o] = (mixrel[o].astype(F32) * factor * gainrel[o, 0:1, :]).astype(BF)
+    for n in range(NC):
+        if n > 0:
+            with jax.named_scope(f"pass{n}"):
+                pass_on(n)
+            if n + 2 < NC:
+                for kind in (0, 1):
+                    start(acopy(kind, n + 2))
+        with jax.named_scope(f"ring{n}"):
+            acopy(2, n).wait_recv()
+            acopy(3, n).wait_recv()
+            start(acopy(6, n))
+            for kind in (4, 5, 6):
+                acopy(kind, n).wait_recv()
+        with jax.named_scope(f"proj{n}"):
+            cols = cols_of(n)
+            total = rin[:, cols].astype(F32) + jnp.dot(normed[0], ow[:, cols], preferred_element_type=F32)
+            for o in range(1, ntp):
+                total = total + jnp.dot(normed[o], wrel[o, :, cols], preferred_element_type=F32)
+            res_ref[:, cols] = total.astype(BF)
+        for d in (0, 1):
+            start(zcopy(0, d, n))
 
     def meta_of(offset):
         return meta_ref if offset == 0 else metas.at[offset]
@@ -229,11 +407,20 @@
         rows = count * grp
         base = first * grp
 
+        def norm(i, carry):
+            from_rows = pl.ds(pl.multiple_of(base + i * 32, 32), 32)
+            vals = arrived[from_rows, :].astype(F32)
+            factor = lax.rsqrt(jnp.mean(vals * vals, axis=1, keepdims=True) + EPSILON)
+            act[pl.ds(pl.multiple_of(i * 32, 32), 32), :] = (vals * factor * mgain_ref[...].astype(F32)).astype(BF)
+            return carry
+
+        lax.fori_loop(0, rows // 32, norm, 0)
+
         def up(f, carry):
             cols = pl.ds(pl.multiple_of(f * fw, fw), fw)
-            act = arrived[base : base + rows, :]
-            g = jnp.dot(act, wg[:, cols], preferred_element_type=F32)
-            u = jnp.dot(act, wu[:, cols], preferred_element_type=F32)
+            x = act[0:rows, :]
+            g = jnp.dot(x, wg[:, cols], preferred_element_type=F32)
+            u = jnp.dot(x, wu[:, cols], preferred_element_type=F32)
             hid[0:rows, cols] = (g * jax.nn.sigmoid(g) * u).astype(BF)
             return carry
 
@@ -248,7 +435,7 @@
         lax.fori_loop(0, NC, down, 0)
 
     with jax.named_scope("own"):
-        pack(0, 0, rows_ref)
+        pack(0, 0, res_ref)
         xstart(0)
     for n, d in both:
         with jax.named_scope(f"hop1_{n}{d}"):
@@ -402,16 +589,49 @@
         wait_bytes(ref, sem)
 
 
-def moe(rows, res, meta, wg, wu, wd):
-    tok, width = rows.shape
-    fe = wg.shape[2]
+def body(
+    residual_in,
+    gate_outer,
+    gate_inner,
+    conv_input,
+    conv_taps,
+    norm_gain,
+    out_weight,
+    moe_gain,
+    expert_ids,
+    group_prob,
+    route_prob,
+    expert_gate,
+    expert_up,
+    expert_down,
+):
+    tok, width = residual_in.shape
+    seq, chan = conv_input.shape
+    fe = expert_gate.shape[2]
+    ntp = lax.axis_size("tp")
     nj = lax.axis_size("sp") // NZ
     grp = nj * CAP
     vmem = pl.BlockSpec(memory_space=pltpu.VMEM)
     hbm = pl.BlockSpec(memory_space=pl.ANY)
     dma = pltpu.SemaphoreType.DMA
     shapes = [
-        ((NZ,) + meta.shape, F32),
+        ((tok, width), BF),
+        ((seq, chan), BF),
+        ((seq, chan), BF),
+        ((seq, chan), BF),
+        ((chan, width), BF),
+        ((2, 16, chan), BF),
+        ((seq + 8, chan), F32),
+        ((seq, chan), BF),
+        ((ntp, tok, chan), BF),
+        ((8, chan), F32),
+        ((ntp, 8, chan), F32),
+        ((ntp, tok, chan), BF),
+        ((ntp, chan, width), BF),
+        ((tok, width), BF),
+        ((8, tok), F32),
+        ((2 * grp, width), BF),
+        ((NZ, 8, tok), F32),
         ((2, tok, width), BF),
         ((2, tok, width), BF),
         ((2, grp, tok), BF),
@@ -437,93 +657,39 @@
         ((2, tok, width), BF),
         ((2, tok, width), BF),
         ((2 * grp, fe), BF),
-        (wg.shape[1:], BF),
-        (wu.shape[1:], BF),
-        (wd.shape[1:], BF),
+        ((width, fe), BF),
+        ((width, fe), BF),
+        ((fe, width), BF),
     ]
-    sems = [(3,), (NZ,), (NZ,), (5, 2, NC), (5, 2, NC), (5,), (5,), (5,), (5,)]
+    sems = [(5,), (3,), (2,), (2,), (2, ntp), (2, ntp), (7, NC), (7, NC)]
+    sems += [(NZ,), (NZ,), (5, 2, NC), (5, 2, NC), (5,), (5,), (5,), (5,)]
     sems += [(2, 2, NC), (2, 2, NC), (2, 2, NC), (2, 2, NC), (5, 2, NC), (5, 2, NC)]
     return pl.pallas_call(
-        moe_kernel,
+        layer_kernel,
         out_shape=jax.ShapeDtypeStruct((tok, width), BF),
-        in_specs=[vmem, vmem, vmem, hbm, hbm, hbm],
+        in_specs=[hbm] * 8 + [vmem] * 6,
         out_specs=vmem,
         scratch_shapes=[pltpu.VMEM(s, t) for s, t in shapes] + [dma(s) for s in sems],
         compiler_params=pltpu.CompilerParams(
-            collective_id=0, has_side_effects=True, vmem_limit_bytes=60 * 1024 * 1024
+            collective_id=0, has_side_effects=True, vmem_limit_bytes=61 * 1024 * 1024
         ),
-        name="moe",
-    )(rows, res, meta, wg, wu, wd)
-
-
-def from_behind(shard, axis, by):
-    devices = lax.axis_size(axis)
-    pairs = [(i, i + by) for i in range(devices) if 0 <= i + by < devices]
-    return lax.ppermute(shard, axis, pairs)
-
-
-def rms_norm(values, gain):
-    floats = values.astype(F32)
-    factor = lax.rsqrt(jnp.mean(floats * floats, axis=-1, keepdims=True) + EPSILON)
-    return floats * factor * gain.astype(F32)
-
-
-def slot_meta(expert_ids, group_prob, route_prob, experts_all):
-    tok = expert_ids.shape[0]
-    lane = jnp.arange(experts_all, dtype=jnp.int32)[None, :]
-    hot0 = (expert_ids[:, 0:1] == lane).astype(BF)
-    hot1 = (expert_ids[:, 1:2] == lane).astype(BF)
-    row = jnp.arange(tok, dtype=jnp.int32)
-    before = (row[:, None] > row[None, :]).astype(BF)
-    ranks = jnp.dot(before, jnp.concatenate([hot0, hot1], axis=1), preferred_element_type=F32)
-    count0 = jnp.sum(hot0.astype(F32), axis=0, keepdims=True)
-    rank0 = jnp.sum(ranks[:, :experts_all] * hot0, axis=1)
-    rank1 = jnp.sum((ranks[:, experts_all:] + count0) * hot1, axis=1)
-    pos0 = expert_ids[:, 0].astype(F32) * CAP + rank0
-    pos1 = expert_ids[:, 1].astype(F32) * CAP + rank1
-    weights = group_prob[:, None] * route_prob / jnp.sum(route_prob, axis=1, keepdims=True)
-    zero = jnp.zeros_like(pos0)
-    return jnp.stack([pos0, pos1, weights[:, 0], weights[:, 1], zero, zero, zero, zero], axis=0)
-
-
-def body(
-    residual_in,
-    gate_outer,
-    gate_inner,
-    conv_input,
-    conv_taps,
-    norm_gain,
-    out_weight,
-    moe_gain,
-    expert_ids,
-    group_prob,
-    route_prob,
-    expert_gate,
-    expert_up,
-    expert_down,
-):
-    seq_rows, channels = conv_input.shape
-    taps_count = conv_taps.shape[0]
-    inner = gate_inner.astype(F32) * conv_input.astype(F32)
-    earlier = from_behind(inner[seq_rows - (taps_count - 1) :], "sp", 1)
-    padded = jnp.concatenate([earlier, inner], axis=0)
-    tap_f = conv_taps.astype(F32)
-    filtered = jnp.zeros((seq_rows, channels), F32)
-    for offset in range(taps_count):
-        filtered = filtered + tap_f[offset][None, :] * padded[offset : offset + seq_rows]
-    mixed_out = (gate_outer.astype(F32) * filtered).astype(BF)
-    gathered = lax.all_to_all(mixed_out, "tp", split_axis=0, concat_axis=1, tiled=True)
-    full_weight, full_gain = (
-        lax.all_gather(out_weight, "tp", axis=0, tiled=True),
-        lax.all_gather(norm_gain, "tp", axis=0, tiled=True),
+        name="layer",
+    )(
+        residual_in,
+        gate_outer,
+        gate_inner,
+        conv_input,
+        out_weight,
+        expert_gate,
+        expert_up,
+        expert_down,
+        conv_taps,
+        norm_gain.reshape(1, chan),
+        moe_gain.reshape(1, width),
+        expert_ids.T,
+        group_prob.reshape(1, tok),
+        route_prob.T,
     )
-    normed = rms_norm(gathered, full_gain).astype(BF)
-    projected = jnp.dot(normed, full_weight, preferred_element_type=F32)
-    residual = (residual_in.astype(F32) + projected).astype(BF)
-    routed_in = rms_norm(residual, moe_gain).astype(BF)
-    experts_all = expert_gate.shape[0] * lax.axis_size("sp")
-    meta = slot_meta(expert_ids, group_prob, route_prob, experts_all)
-    return moe(routed_in, residual, meta, expert_gate, expert_up, expert_down)
 
 
 def solution(mesh):

time: 238 us -> 184 us (0.77)
  waiting for transfers between devices: 32.3 us -> 0 us
  Pallas kernels: 159 us -> 179 us
  between operations: 13.6 us -> 0.01 us
  blocking collectives: 11.4 us -> 0 us
  starting transfers between devices: 8.72 us -> 0 us
  other arithmetic: 4.56 us -> 0 us
  matrix products: 4.1 us -> 0 us
    all_gather x1 -> x0, waiting for transfers between devices: 31.3 us -> none  [body(): lax.all_gather(out_weight, 'tp', axis=0, tiled=True)]
    pallas_call x1, Pallas kernels: 159 us -> 179 us  [body(): pl.pallas_call(layer_kernel, out_shape=jax.ShapeDtypeStruct((tok, width),...]
    all_gather x1 -> x0, blocking collectives: 11.4 us -> none  [body(): lax.all_gather(norm_gain, 'tp', axis=0, tiled=True)]
    ppermute x1 -> x0, starting transfers between devices: 4.5 us -> none  [from_behind(): return lax.ppermute(shard, axis, pairs)]
    all_to_all x1 -> x0, starting transfers between devices: 4.18 us -> none  [body(): lax.all_to_all(mixed_out, 'tp', split_axis=0, concat_axis=1, tiled=True)]
    dot_general x2 -> x0, matrix products: 4.1 us -> none  [the longest x1 3.9 us: body(): projected = jnp.dot(normed, full_weight, preferred_element_type=F32)]
    convert_element_type x7 -> x0, other arithmetic: 2.81 us -> none  [the longest x1 1.3 us: body(): routed_in = rms_norm(residual, moe_gain).astype(BF)]
    reshape x0 -> x2, local copies, waits for them, and re-layouts: none -> 2.53 us  [the longest x1 1.29 us: body(): moe_gain.reshape(1, width)]
  transfers between devices with their start and end apart: 3 -> 0, of which waited for: 2 -> 0; matrix products, arithmetic and copies ran while one was open for 2% -> 0% of each run, Pallas kernels for 0% -> 0%
where the time goes in v3:
time: 184 us
  Pallas kernels  179 us (97%)
  local copies, waits for them, and re-layouts  4.84 us (3%)
    pallas_call x1, Pallas kernels, body(): pl.pallas_call(layer_kernel, out_shape=jax.ShapeDtypeStruct((tok, width),...  179 us

profile of v3, /device:TPU:1, one launch (start us, length us, event | category | flops | bytes accessed | tf_op | source)
XLA Modules:
  0.0 184.1 jit_solution(9058448725729590838)
XLA Ops:
  0.0 1.2 reshape.9.gain_ref
  1.2 1.3 reshape.10.mgain_ref
  2.5 179.3 %layer.1 = bf16[256,2048]{1,0:T(8,128)(2,1)} custom-call(bf16[256,2048]{1,0:T(8,128)(2,1)} %rin_hbm.1, bf16[1024,256]{1,0:T(8,128)(2,1)} %go_hbm.1, bf16[1024,256]{1,0:T(8,128)(2,1)} %gi_hbm.1, bf16[1024,256]{1,0:T(8,128)(2,1)} %ci_hbm.1, bf16[256,2048]{1,0:T(8,128)(2,1)} %ow_hbm.1, bf16[1,2048,512]{2,1,0:T(8,128)(2,1)} %wg_hbm.1, ...), custom_call_target="tpu_custom_call" | custom-call | tf_op jit(solution)/shard_map/layer/pallas_call | solution.py:667
  181.8 2.3 %copy.16 = bf16[256,2048]{1,0:T(8,128)(2,1)} copy(bf16[256,2048]{1,0:T(8,128)(2,1)} %layer.1) | data formatting | bytes 2097152

commit v4 on v3

v4 whole, which is shorter than its diff:
```python
import jax
import jax.numpy as jnp
from jax import lax
from jax.experimental import pallas as pl
from jax.experimental.pallas import tpu as pltpu
from jax.sharding import PartitionSpec as P

EPSILON = 1e-06
NZ = 8
CAP = 16
NC = 4
MESH = pl.DeviceIdType.MESH
BF = jnp.bfloat16
F32 = jnp.float32


def layer_kernel(
    rin_hbm,
    go_hbm,
    gi_hbm,
    ci_hbm,
    ow_hbm,
    wg_hbm,
    wu_hbm,
    wd_hbm,
    taps_ref,
    gain_ref,
    mgain_ref,
    ids_ref,
    group_ref,
    route_ref,
    out_ref,
    rin,
    go,
    gi,
    ci,
    ow,
    halo,
    inner,
    mixed,
    mixrel,
    gainsrc,
    gainrel,
    normed,
    normed_near,
    wrel,
    res_ref,
    meta_ref,
    squares,
    gate,
    value,
    mgain,
    out,
    sel,
    metas,
    hop1,
    hop2,
    sel3,
    sel4,
    pack3,
    pack4,
    gather3,
    gather4,
    pass4,
    packed,
    arrived,
    results,
    ret0,
    ret1,
    ret2,
    got3,
    back4,
    got4,
    ret3,
    ret4,
    send2,
    part2,
    send1,
    part1,
    hid,
    wg,
    wu,
    wd,
    isem,
    osem,
    wsem,
    ssem,
    trecv,
    arecv,
    nrecv,
    mrecv,
    zrecv,
    xrecv,
    yrecv,
    grecv,
    brecv,
    rrecv,
):
    tok, width = res_ref.shape
    nsp = lax.axis_size("sp")
    ntp = lax.axis_size("tp")
    nj = nsp // NZ
    grp = nj * CAP
    seq, chan = mixed.shape
    others = grp - CAP
    cw = width // NC
    hw = cw // 2
    sp = lax.axis_index("sp")
    tp = lax.axis_index("tp")
    z = sp // nj
    me_j = sp % nj
    step = (1, -1)
    near = (1, NZ - 1)
    far = (2, NZ - 2)
    both = [(n, d) for n in range(NC) for d in (0, 1)]

    def zval(offset):
        return lax.rem(z + offset + NZ, NZ)

    def zid(offset):
        return (zval(offset) * nj + me_j, tp)

    def jid(offset):
        return (z * nj + lax.rem(me_j + offset, nj), tp)

    def tid(offset):
        return (sp, lax.rem(tp + offset, ntp))

    after = (lax.rem(sp + 1, nsp), tp)
    before = (lax.rem(sp + nsp - 1, nsp), tp)
    core = lax.rem(me_j, 2)
    partner = (z * nj + me_j + 1 - 2 * core, tp)

    def cols_of(n):
        return slice(n * cw, (n + 1) * cw)

    def half_of(n):
        return slice(n * hw, (n + 1) * hw)

    def part_of(n, d):
        return slice(n * cw + d * hw, n * cw + (d + 1) * hw)

    def slot_rows(b, j):
        return pl.ds(pl.multiple_of(b * grp + j * CAP, CAP), CAP)

    def block_rows(b):
        return slice(b * grp, (b + 1) * grp)

    near_z, far_z, back_near, back_far, xs, ys, gs, bs, ring, rows_t, gains_t, halo_t, metas_z, normed_z = range(14)

    def remote(src, dst, send, recv, device):
        return pltpu.make_async_remote_copy(
            src_ref=src, dst_ref=dst, send_sem=send, recv_sem=recv, device_id=device, device_id_type=MESH
        )

    def wait_bytes(ref, sem):
        pltpu.make_async_copy(ref, ref, sem).wait()

    def make_slots():
        expert = lax.broadcasted_iota(jnp.int32, (nsp, tok), 0)
        hot = [jnp.where(expert == ids_ref[k : k + 1, :], 1.0, 0.0) for k in (0, 1)]
        earlier_tok = lax.broadcasted_iota(jnp.int32, (tok, tok), 0) < lax.broadcasted_iota(jnp.int32, (tok, tok), 1)
        upper = jnp.where(earlier_tok, 1.0, 0.0).astype(BF)
        rank = [jnp.dot(h.astype(BF), upper, preferred_element_type=F32) for h in hot]
        count = jnp.sum(hot[0], axis=1, keepdims=True)
        slot = expert.astype(F32) * CAP
        meta_ref[0:1, :] = jnp.sum((rank[0] + slot) * hot[0], axis=0, keepdims=True)
        meta_ref[1:2, :] = jnp.sum((rank[1] + count + slot) * hot[1], axis=0, keepdims=True)
        meta_ref[2:3, :] = group_ref[...] * route_ref[0:1, :] / (route_ref[0:1, :] + route_ref[1:2, :])
        meta_ref[3:4, :] = group_ref[...] * route_ref[1:2, :] / (route_ref[0:1, :] + route_ref[1:2, :])
        meta_ref[4:8, :] = jnp.zeros((4, tok), F32)

    icopies = [
        pltpu.make_async_copy(src, dst, isem.at[i])
        for i, (src, dst) in enumerate(((ow_hbm, ow), (rin_hbm, rin), (gi_hbm, gi), (ci_hbm, ci), (go_hbm, go)))
    ]
    wcopies = [
        pltpu.make_async_copy(wg_hbm.at[0], wg, wsem.at[0]),
        pltpu.make_async_copy(wu_hbm.at[0], wu, wsem.at[1]),
        pltpu.make_async_copy(wd_hbm.at[0], wd, wsem.at[2]),
    ]
    barrier = pltpu.get_barrier_semaphore()
    for offset in (1, -1):
        pl.semaphore_signal(barrier, inc=1, device_id=zid(offset), device_id_type=MESH)
    for offset in range(1, nj):
        pl.semaphore_signal(barrier, inc=1, device_id=jid(offset), device_id_type=MESH)
    for offset in range(1, ntp):
        pl.semaphore_signal(barrier, inc=1, device_id=tid(offset), device_id_type=MESH)
    for ident in (after, before):
        pl.semaphore_signal(barrier, inc=1, device_id=ident, device_id_type=MESH)
    for copy in icopies:
        copy.start()
    make_slots()
    with jax.named_scope("barrier"):
        pl.semaphore_wait(barrier, nj + ntp + 2)

    def mcopy(hop, d):
        src = metas.at[near[d]] if hop else meta_ref
        dst = metas.at[far[d] if hop else near[d]]
        return remote(src, dst, ssem.at[metas_z], mrecv.at[hop, d], zid(step[d]))

    def zcopy(hop, d, n):
        cols = cols_of(n)
        if hop == 0:
            src, dst = rin.at[:, cols], hop1.at[d, :, cols]
        elif hop == 1:
            src, dst = hop1.at[d, :, cols], hop2.at[d, :, cols]
        elif hop == 2:
            src, dst = gather3.at[d, :, cols], arrived.at[block_rows(5 + d), cols]
        elif hop == 3:
            src, dst = gather4.at[d, :, half_of(n)], pass4.at[d, :, half_of(n)]
        else:
            src, dst = pass4.at[d, :, half_of(n)], arrived.at[block_rows(7), part_of(n, d)]
        return remote(src, dst, ssem.at[near_z if hop < 2 else far_z], zrecv.at[hop, d, n], zid(step[d]))

    def meta_of(offset):
        return meta_ref if offset == 0 else metas.at[offset]

    def slots_of(target):
        return (lax.broadcasted_iota(jnp.int32, (grp, tok), 0) + target * grp).astype(F32)

    def select(offset, target):
        ref = meta_of(offset)
        slot = slots_of(target)
        hit = jnp.where(slot == ref[0:1, :], 1.0, 0.0) + jnp.where(slot == ref[1:2, :], 1.0, 0.0)
        return hit.astype(BF)

    def spread(offset, target):
        ref = meta_of(offset)
        slot = slots_of(target)
        hit = jnp.where(slot == ref[0:1, :], ref[2:3, :], 0.0) + jnp.where(slot == ref[1:2, :], ref[3:4, :], 0.0)
        return hit.astype(BF)

    def combine(weights, rows):
        return lax.dot_general(weights, rows, (((0,), (0,)), ((), ())), preferred_element_type=F32)

    def ytarget(b):
        return ret0 if b == 0 else ret1.at[b - 1] if b < 3 else ret2.at[b - 3]

    def xstart(b, n):
        cols = cols_of(n)
        for offset in range(1, nj):
            their = slot_rows(0, lax.rem(me_j + offset, nj))
            src, dst = packed.at[b, their, cols], arrived.at[slot_rows(b, me_j), cols]
            remote(src, dst, ssem.at[xs], xrecv.at[b], jid(offset)).start()
        arrived[slot_rows(b, me_j), cols] = packed[b, slot_rows(0, me_j), cols]

    def xwait(b):
        wait_bytes(arrived.at[b * grp : b * grp + others, :], xrecv.at[b])

    def ystart(b):
        dst = ytarget(b)
        for offset in range(1, nj):
            their = slot_rows(b, lax.rem(me_j + offset, nj))
            remote(results.at[their, :], dst.at[slot_rows(0, me_j), :], ssem.at[ys], yrecv.at[b], jid(offset)).start()
        dst[slot_rows(0, me_j), :] = results[slot_rows(b, me_j), :]

    def ywait(b):
        wait_bytes(ytarget(b).at[0:others, :], yrecv.at[b])

    def exchange(src, dst, d, cols, send, recv):
        mine = slot_rows(0, me_j)
        for offset in range(1, nj):
            their = slot_rows(0, lax.rem(me_j + offset, nj))
            remote(src.at[d, their, cols], dst.at[d, mine, cols], send, recv, jid(offset)).start()
        dst[d, mine, cols] = src[d, mine, cols]

    def pack(b, block, n, go_now=True):
        cols = cols_of(n)
        packed[b, :, cols] = jnp.dot(sel[b], block[:, cols], preferred_element_type=F32).astype(BF)
        if go_now:
            xstart(b, n)

    def own_cols(n):
        return pl.ds(pl.multiple_of(n * cw + core * hw, hw), hw)

    def quarter_cols(n, d):
        return pl.ds(pl.multiple_of(n * cw + core * hw + d * (hw // 2), hw // 2), hw // 2)

    def acopy(kind, n):
        if kind == 0:
            src, dst, device = ow.at[:, own_cols(n)], wrel.at[3, :, own_cols(n)], tid(1)
        elif kind == 1:
            src, dst, device = ow.at[:, own_cols(n)], wrel.at[1, :, own_cols(n)], tid(ntp - 1)
        elif kind == 2:
            cols = quarter_cols(n, 0)
            src, dst, device = wrel.at[3, :, cols], wrel.at[2, :, cols], tid(1)
        elif kind == 3:
            cols = quarter_cols(n, 1)
            src, dst, device = wrel.at[1, :, cols], wrel.at[2, :, cols], tid(ntp - 1)
        else:
            cols = own_cols(n)
            block = (3, 1, 2)[kind - 4]
            src, dst, device = wrel.at[block, :, cols], wrel.at[block, :, cols], partner
        return remote(src, dst, ssem.at[ring], arecv.at[(0, 1, 2, 2, 3, 3, 3)[kind], n], device)

    def tcopy(offset):
        rows = pl.ds(pl.multiple_of(lax.rem(tp + offset, ntp) * tok, tok), tok)
        return remote(mixed.at[rows, :], mixrel.at[ntp - offset], ssem.at[rows_t], trecv.at[0], tid(offset))

    def gcopy(offset):
        return remote(gainsrc, gainrel.at[ntp - offset], ssem.at[gains_t], trecv.at[1], tid(offset))

    def hcopy(i):
        src = (gi_hbm, ci_hbm)[i]
        return remote(src.at[seq - 16 : seq, :], halo.at[i], ssem.at[halo_t], trecv.at[2], after)

    def pass_on(n):
        acopy(0, n).wait_recv()
        acopy(2, n).start()
        acopy(4, n).start()
        acopy(1, n).wait_recv()
        acopy(3, n).start()
        acopy(5, n).start()

    for i in (0, 1):
        hcopy(i).start()
    for d in (0, 1):
        mcopy(0, d).start()
    with jax.named_scope("inputs"):
        icopies[0].wait()
    for kind in (0, 1):
        acopy(kind, 0).start()
    with jax.named_scope("rin"):
        icopies[1].wait()
    for n in range(NC - 1):
        for d in (0, 1):
            zcopy(0, d, n).start()
    mgain[...] = jnp.broadcast_to(mgain_ref[...].astype(F32)[None, :], mgain.shape)
    gainsrc[...] = jnp.broadcast_to(gain_ref[...].astype(F32)[None, :], gainsrc.shape)
    for offset in range(1, ntp):
        gcopy(offset).start()
    for i in (2, 3, 4):
        icopies[i].wait()
    for copy in wcopies:
        copy.start()
    taps = taps_ref[...].astype(F32)
    kw = taps_ref.shape[0]
    with jax.named_scope("conv"):
        inner[8 : 8 + seq, :] = gi[...].astype(F32) * ci[...].astype(F32)

        def mix(first, rows):
            filtered = taps[0:1, :] * inner[9 - kw + first : 9 - kw + first + rows, :]
            for k in range(1, kw):
                filtered = filtered + taps[k : k + 1, :] * inner[9 - kw + k + first : 9 - kw + k + first + rows, :]
            mixed[first : first + rows, :] = (go[first : first + rows, :].astype(F32) * filtered).astype(BF)

        mix(tok, seq - tok)
    for offset in range(1, ntp):
        pl.when(lax.rem(tp + offset, ntp) != 0)(tcopy(offset).start)
    with jax.named_scope("pass0"):
        pass_on(0)
    with jax.named_scope("halo"):
        wait_bytes(halo, trecv.at[2])
    earlier = halo[0, 8:16, :].astype(F32) * halo[1, 8:16, :].astype(F32)
    inner[0:8, :] = jnp.where(sp > 0, earlier, 0.0)
    mix(0, tok)
    for offset in range(1, ntp):
        pl.when(lax.rem(tp + offset, ntp) == 0)(tcopy(offset).start)
    mixrel[0] = mixed[pl.ds(pl.multiple_of(tp * tok, tok), tok), :]

    with jax.named_scope("rows"):
        wait_bytes(mixrel.at[1:ntp], trecv.at[0])
        wait_bytes(gainrel.at[1:ntp], trecv.at[1])
    gainrel[0] = gainsrc[...]
    for n in (1, 2):
        for kind in (0, 1):
            acopy(kind, n).start()
    with jax.named_scope("norm"):
        square = jnp.zeros((tok, 1), F32)
        for o in range(ntp):
            part = mixrel[o].astype(F32)
            square = square + jnp.sum(part * part, axis=1, keepdims=True)
        factor = lax.rsqrt(square / (chan * ntp) + EPSILON)
        for o in range(ntp):
            normed[o] = (mixrel[o].astype(F32) * factor * gainrel[o, 0:1, :]).astype(BF)

    def ncopy(d):
        return remote(normed, normed_near.at[d], ssem.at[normed_z], nrecv.at[d], zid(step[d]))

    for d in (0, 1):
        ncopy(d).start()
    for d in (0, 1):
        zcopy(0, d, NC - 1).start()

    def selections():
        sel[0] = select(0, z)
        for d in (0, 1):
            mcopy(0, d).wait_recv()
            mcopy(1, d).start()
            sel[1 + d] = select(near[d], z)

    def far_selections():
        for d in (0, 1):
            mcopy(1, d).wait_recv()
            sel[3 + d] = select(far[d], z)
            sel3[d] = select(far[d], zval(step[d]))
            sel4[d] = select(far[d], zval(2 * step[d]))

    def project(values, rows, n):
        cols = cols_of(n)
        total = values[:, cols].astype(F32) + jnp.dot(rows[0], ow[:, cols], preferred_element_type=F32)
        for o in range(1, ntp):
            total = total + jnp.dot(rows[o], wrel[o, :, cols], preferred_element_type=F32)
        return total.astype(BF)

    for n in range(NC):
        with jax.named_scope(f"ring{n}"):
            wait_bytes(wrel.at[2, :, 0:hw], arecv.at[2, n])
            acopy(6, n).start()
            wait_bytes(wrel.at[1:4, :, 0:hw], arecv.at[3, n])
        with jax.named_scope(f"proj{n}"):
            res_ref[:, cols_of(n)] = project(rin, normed, n)
        if n == 0:
            with jax.named_scope("selections"):
                selections()
        with jax.named_scope(f"own{n}"):
            pack(0, res_ref, n)
        for later in ((1, 2), (3,), (), ())[n]:
            with jax.named_scope(f"pass{later}"):
                pass_on(later)
            if later == 1:
                for kind in (0, 1):
                    acopy(kind, 3).start()

    def expert_in(first, count, n, fresh):
        rows = count * grp
        base = first * grp
        cols = pl.ds(pl.multiple_of(n * cw, cw), cw)
        vals = arrived[base : base + rows, cols].astype(F32)
        x = (vals * mgain[0:1, cols]).astype(BF)
        parts = jnp.sum(vals * vals, axis=1, keepdims=True)
        g = jnp.dot(x, wg[cols, :], preferred_element_type=F32)
        u = jnp.dot(x, wu[cols, :], preferred_element_type=F32)
        if fresh:
            squares[0:rows, :] = jnp.broadcast_to(parts, (rows, 128))
            gate[0:rows, :] = g
            value[0:rows, :] = u
        else:
            squares[0:rows, :] += jnp.broadcast_to(parts, (rows, 128))
            gate[0:rows, :] += g
            value[0:rows, :] += u

    def expert_mid(count):
        rows = count * grp
        factor = lax.rsqrt(squares[0:rows, 0:1] / width + EPSILON)
        g = gate[0:rows, :] * factor
        hid[0:rows, :] = (g * jax.nn.sigmoid(g) * (value[0:rows, :] * factor)).astype(BF)

    def expert_out(first, count, n):
        rows = count * grp
        cols = pl.ds(pl.multiple_of(n * cw, cw), cw)
        r = jnp.dot(hid[0:rows, :], wd[:, cols], preferred_element_type=F32)
        results[first * grp : first * grp + rows, cols] = r.astype(BF)

    def experts(first, count):
        expert_in(first, count, 0, True)

        def more(n, carry):
            expert_in(first, count, n, False)
            return carry

        lax.fori_loop(1, NC, more, 0)
        expert_mid(count)

        def out_cols(n, carry):
            expert_out(first, count, n)
            return carry

        lax.fori_loop(0, NC, out_cols, 0)

    with jax.named_scope("normed"):
        for d in (0, 1):
            ncopy(d).wait_recv()
    for n, d in both:
        with jax.named_scope(f"hop1_{n}{d}"):
            zcopy(0, d, n).wait_recv()
        hop1[d, :, cols_of(n)] = project(hop1.at[d], normed_near.at[d], n)
        zcopy(1, d, n).start()
        pack(1 + d, hop1.at[d], n)
    with jax.named_scope("far_selections"):
        far_selections()
    for copy in wcopies:
        copy.wait()
    xwait(0)
    with jax.named_scope("exp0"):
        experts(0, 1)

    def hop3_out(n):
        for d in (0, 1):
            with jax.named_scope(f"ex{n}{d}"):
                wait_bytes(gather3.at[d, 0:others, 0 : cw + hw], grecv.at[d, n])
            zcopy(3, d, n).start()
            zcopy(2, d, n).start()

    for n in range(NC):
        for d in (0, 1):
            with jax.named_scope(f"hop2_{n}{d}"):
                zcopy(1, d, n).wait_recv()
            part = hop2[d, :, cols_of(n)]
            pack3[d, :, cols_of(n)] = jnp.dot(sel3[d], part, preferred_element_type=F32).astype(BF)
            part = hop2[d, :, part_of(n, d)]
            pack4[d, :, half_of(n)] = jnp.dot(sel4[d], part, preferred_element_type=F32).astype(BF)
            exchange(pack4, gather4, d, half_of(n), ssem.at[gs], grecv.at[d, n])
            exchange(pack3, gather3, d, cols_of(n), ssem.at[gs], grecv.at[d, n])
            pack(3 + d, hop2.at[d], n, False)
        if n > 0:
            hop3_out(n - 1)
            xstart(3, n - 1)
            xstart(4, n - 1)
        if n == 1:
            xwait(1)
            xwait(2)
            with jax.named_scope("exp12"):
                experts(1, 2)
    hop3_out(NC - 1)
    xstart(3, NC - 1)
    xstart(4, NC - 1)

    def rcopy(kind, d, n):
        cols = cols_of(n)
        if kind == 0:
            src, dst = results.at[block_rows(7), part_of(n, d)], back4.at[d, :, half_of(n)]
        elif kind == 1:
            src, dst = results.at[block_rows(5 + d), cols], got3.at[d, :, cols]
        elif kind == 2:
            src, dst = back4.at[d, :, half_of(n)], got4.at[d, :, half_of(n)]
        elif kind == 3:
            src, dst = send2.at[d, :, cols], part2.at[d, :, cols]
        else:
            src, dst = send1.at[d, :, cols], part1.at[d, :, cols]
        return remote(src, dst, ssem.at[back_near if kind > 2 else back_far], rrecv.at[kind, d, n], zid(-step[d]))

    for n in range(NC):
        for d in (0, 1):
            with jax.named_scope(f"hop3_{n}{d}"):
                zcopy(3, d, n).wait_recv()
            zcopy(4, d, n).start()
        with jax.named_scope(f"hop3w{n}"):
            for d in (0, 1):
                zcopy(2, d, n).wait_recv()
        with jax.named_scope(f"in56_{n}"):
            expert_in(5, 2, n, n == 0)
    with jax.named_scope("out56"):
        expert_mid(2)
        for n in range(NC):
            expert_out(5, 2, n)
            for d in (0, 1):
                rcopy(1, d, n).start()
    with jax.named_scope("xw34"):
        xwait(3)
        xwait(4)
    with jax.named_scope("exp34"):
        experts(3, 2)
    ystart(3)
    ystart(4)
    for n in range(NC):
        with jax.named_scope(f"hop4w{n}"):
            for d in (0, 1):
                zcopy(4, d, n).wait_recv()
        with jax.named_scope(f"in7_{n}"):
            expert_in(7, 1, n, n == 0)
    with jax.named_scope("out7"):
        expert_mid(1)
        for n in range(NC):
            expert_out(7, 1, n)
            for d in (0, 1):
                rcopy(0, d, n).start()
    for n, d in both:
        with jax.named_scope(f"r3_{n}{d}"):
            rcopy(1, d, n).wait_recv()
        exchange(got3, ret3, d, cols_of(n), ssem.at[bs], brecv.at[d, n])
    for n, d in both:
        with jax.named_scope(f"r4_{n}{d}"):
            rcopy(0, d, n).wait_recv()
        rcopy(2, d, n).start()
    ywait(3)
    ywait(4)

    def sums2_out(n):
        for d in (0, 1):
            with jax.named_scope(f"ex{n}{d}"):
                wait_bytes(ret3.at[d, 0:others, 0 : cw + hw], brecv.at[d, n])
            total = combine(spread(far[d], z), ret2[d, :, cols_of(n)])
            total = total + combine(spread(far[d], zval(step[d])), ret3[d, :, cols_of(n)])
            last = combine(spread(far[d], zval(2 * step[d])), ret4[d, :, half_of(n)])
            lo, hi = total[:, :hw], total[:, hw:]
            if d == 0:
                lo = lo + last
            else:
                hi = hi + last
            send2[d, :, part_of(n, 0)] = lo.astype(BF)
            send2[d, :, part_of(n, 1)] = hi.astype(BF)
            rcopy(3, d, n).start()

    for n in range(NC):
        for d in (0, 1):
            with jax.named_scope(f"r3b_{n}{d}"):
                rcopy(2, d, n).wait_recv()
            exchange(got4, ret4, d, half_of(n), ssem.at[bs], brecv.at[d, n])
        if n > 0:
            sums2_out(n - 1)
    sums2_out(NC - 1)
    ystart(1)
    ystart(2)
    ystart(0)
    ywait(1)
    ywait(2)
    for n, d in both:
        with jax.named_scope(f"r2_{n}{d}"):
            rcopy(3, d, n).wait_recv()
        cols = cols_of(n)
        total = part2[d, :, cols].astype(F32) + combine(spread(near[d], z), ret1[d, :, cols])
        send1[d, :, cols] = total.astype(BF)
        rcopy(4, d, n).start()
    ywait(0)
    own = spread(0, z)
    ocopies = []
    for n in range(NC):
        with jax.named_scope(f"r1_{n}"):
            rcopy(4, 0, n).wait_recv()
            rcopy(4, 1, n).wait_recv()
        cols = cols_of(n)
        total = res_ref[:, cols].astype(F32) + combine(own, ret0[:, cols])
        total = total + part1[0, :, cols].astype(F32) + part1[1, :, cols].astype(F32)
        out[:, cols] = total.astype(BF)
        copy = pltpu.make_async_copy(out.at[:, cols], out_ref.at[:, cols], osem.at[n])
        copy.start()
        ocopies.append(copy)
    with jax.named_scope("ends"):
        for copy in ocopies:
            copy.wait()
        flat = ((near_z, 4 * tok), (far_z, 4 * grp), (back_near, 4 * tok), (back_far, 4 * grp), (xs, 5 * others), (ys, 5 * others))
        flat += ((gs, 3 * others), (bs, 3 * others), (ring, 3 * chan), (rows_t, 3 * tok * chan // width), (normed_z, 2 * ntp * tok * chan // width))
        for kind, rows in flat:
            wait_bytes(arrived.at[0:rows, :], ssem.at[kind])
        wait_bytes(gainrel.at[1:ntp], ssem.at[gains_t])
        wait_bytes(halo, ssem.at[halo_t])
        wait_bytes(metas.at[0:4], ssem.at[metas_z])


def body(
    residual_in,
    gate_outer,
    gate_inner,
    conv_input,
    conv_taps,
    norm_gain,
    out_weight,
    moe_gain,
    expert_ids,
    group_prob,
    route_prob,
    expert_gate,
    expert_up,
    expert_down,
):
    tok, width = residual_in.shape
    seq, chan = conv_input.shape
    fe = expert_gate.shape[2]
    ntp = lax.axis_size("tp")
    nj = lax.axis_size("sp") // NZ
    grp = nj * CAP
    vmem = pl.BlockSpec(memory_space=pltpu.VMEM)
    hbm = pl.BlockSpec(memory_space=pl.ANY)
    dma = pltpu.SemaphoreType.DMA
    shapes = [
        ((tok, width), BF),
        ((seq, chan), BF),
        ((seq, chan), BF),
        ((seq, chan), BF),
        ((chan, width), BF),
        ((2, 16, chan), BF),
        ((seq + 8, chan), F32),
        ((seq, chan), BF),
        ((ntp, tok, chan), BF),
        ((8, chan), F32),
        ((ntp, 8, chan), F32),
        ((ntp, tok, chan), BF),
        ((2, ntp, tok, chan), BF),
        ((ntp, chan, width), BF),
        ((tok, width), BF),
        ((8, tok), F32),
        ((2 * grp, 128), F32),
        ((2 * grp, fe), F32),
        ((2 * grp, fe), F32),
        ((8, width), F32),
        ((tok, width), BF),
        ((5, grp, tok), BF),
        ((NZ, 8, tok), F32),
        ((2, tok, width), BF),
        ((2, tok, width), BF),
        ((2, grp, tok), BF),
        ((2, grp, tok), BF),
        ((2, grp, width), BF),
        ((2, grp, width // 2), BF),
        ((2, grp, width), BF),
        ((2, grp, width // 2), BF),
        ((2, grp, width // 2), BF),
        ((5, grp, width), BF),
        ((8 * grp, width), BF),
        ((8 * grp, width), BF),
        ((grp, width), BF),
        ((2, grp, width), BF),
        ((2, grp, width), BF),
        ((2, grp, width), BF),
        ((2, grp, width // 2), BF),
        ((2, grp, width // 2), BF),
        ((2, grp, width), BF),
        ((2, grp, width // 2), BF),
        ((2, tok, width), BF),
        ((2, tok, width), BF),
        ((2, tok, width), BF),
        ((2, tok, width), BF),
        ((2 * grp, fe), BF),
        ((width, fe), BF),
        ((width, fe), BF),
        ((fe, width), BF),
    ]
    sems = [(5,), (NC,), (3,), (14,), (3,), (4, NC), (2,), (2, 2), (5, 2, NC), (5,), (5,), (2, NC), (2, NC), (5, 2, NC)]
    return pl.pallas_call(
        layer_kernel,
        out_shape=jax.ShapeDtypeStruct((tok, width), BF),
        in_specs=[hbm] * 8 + [vmem] * 6,
        out_specs=hbm,
        scratch_shapes=[pltpu.VMEM(s, t) for s, t in shapes] + [dma(s) for s in sems],
        compiler_params=pltpu.CompilerParams(
            collective_id=0, has_side_effects=True, vmem_limit_bytes=61 * 1024 * 1024
        ),
        name="layer",
    )(
        residual_in,
        gate_outer,
        gate_inner,
        conv_input,
        out_weight,
        expert_gate,
        expert_up,
        expert_down,
        conv_taps,
        norm_gain,
        moe_gain,
        expert_ids.T,
        group_prob.reshape(1, tok),
        route_prob.T,
    )


def solution(mesh):
    in_specs = (
        P(("sp", "tp"), None),
        P("sp", "tp"),
        P("sp", "tp"),
        P("sp", "tp"),
        P(None, "tp"),
        P("tp"),
        P("tp", None),
        P(),
        P(("sp", "tp"), None),
        P(("sp", "tp")),
        P(("sp", "tp"), None),
        P("sp", None, None),
        P("sp", None, None),
        P("sp", None, None),
    )
    out_specs = P(("sp", "tp"), None)
    return jax.shard_map(body, mesh=mesh, in_specs=in_specs, out_specs=out_specs, check_vma=False)
```

time: 184 us -> 171 us (0.929)
  Pallas kernels: 179 us -> 168 us
  local copies, waits for them, and re-layouts: 4.84 us -> 2.3 us
    pallas_call x1, Pallas kernels: 179 us -> 168 us  [body(): pl.pallas_call(layer_kernel, out_shape=jax.ShapeDtypeStruct((tok, width),...]
    reshape x2 -> x0, local copies, waits for them, and re-layouts: 2.53 us -> none  [the longest x1 1.29 us: body(): moe_gain.reshape(1, width)]
where the time goes in v4:
time: 171 us; the launch traced here: 170 us
  Pallas kernels  168 us (98%)
  local copies, waits for them, and re-layouts  2.3 us (1%)
    pallas_call x1, Pallas kernels, body(): pl.pallas_call(layer_kernel, out_shape=jax.ShapeDtypeStruct((tok, width),...  168 us

profile of v4, /device:TPU:1, one launch (start us, length us, event | category | flops | bytes accessed | tf_op | source)
XLA Modules:
  0.0 170.4 jit_solution(2593492902267786577)
XLA Ops:
  0.0 168.1 %layer.1 = bf16[256,2048]{1,0:T(8,128)(2,1)} custom-call(bf16[256,2048]{1,0:T(8,128)(2,1)} %rin_hbm.1, bf16[1024,256]{1,0:T(8,128)(2,1)} %go_hbm.1, bf16[1024,256]{1,0:T(8,128)(2,1)} %gi_hbm.1, bf16[1024,256]{1,0:T(8,128)(2,1)} %ci_hbm.1, bf16[256,2048]{1,0:T(8,128)(2,1)} %ow_hbm.1, bf16[1,2048,512]{2,1,0:T(8,128)(2,1)} %wg_hbm.1, ...), custom_call_target="tpu_custom_call" | custom-call | tf_op jit(solution)/shard_map/layer/pallas_call | solution.py:721
  168.1 2.3 %copy.16 = bf16[256,2048]{1,0:T(8,128)(2,1)} copy(bf16[256,2048]{1,0:T(8,128)(2,1)} %layer.1) | data formatting | bytes 2097152

commit v5 on v4

--- a/solution.py
+++ b/solution.py
@@ -248,15 +248,21 @@
     def xwait(b):
         wait_bytes(arrived.at[b * grp : b * grp + others, :], xrecv.at[b])
 
-    def ystart(b):
+    def ypart(b, part):
+        return (slice(0, width), b) if b < 3 else (slice(part * (width // 2), (part + 1) * (width // 2)), 3 + 2 * (b - 3) + part)
+
+    def ystart(b, part=0):
         dst = ytarget(b)
+        cols, index = ypart(b, part)
         for offset in range(1, nj):
             their = slot_rows(b, lax.rem(me_j + offset, nj))
-            remote(results.at[their, :], dst.at[slot_rows(0, me_j), :], ssem.at[ys], yrecv.at[b], jid(offset)).start()
-        dst[slot_rows(0, me_j), :] = results[slot_rows(b, me_j), :]
-
-    def ywait(b):
-        wait_bytes(ytarget(b).at[0:others, :], yrecv.at[b])
+            src = results.at[their, cols]
+            remote(src, dst.at[slot_rows(0, me_j), cols], ssem.at[ys], yrecv.at[index], jid(offset)).start()
+        dst[slot_rows(0, me_j), cols] = results[slot_rows(b, me_j), cols]
+
+    def ywait(b, part=0):
+        cols, index = ypart(b, part)
+        wait_bytes(ytarget(b).at[0:others, cols], yrecv.at[index])
 
     def exchange(src, dst, d, cols, send, recv):
         mine = slot_rows(0, me_j)
@@ -506,16 +512,18 @@
             pack(3 + d, hop2.at[d], n, False)
         if n > 0:
             hop3_out(n - 1)
-            xstart(3, n - 1)
-            xstart(4, n - 1)
+            if n < 3:
+                xstart(3, n - 1)
+                xstart(4, n - 1)
         if n == 1:
             xwait(1)
             xwait(2)
             with jax.named_scope("exp12"):
                 experts(1, 2)
     hop3_out(NC - 1)
-    xstart(3, NC - 1)
-    xstart(4, NC - 1)
+    for n in (2, 3):
+        xstart(3, n)
+        xstart(4, n)
 
     def rcopy(kind, d, n):
         cols = cols_of(n)
@@ -536,6 +544,8 @@
             with jax.named_scope(f"hop3_{n}{d}"):
                 zcopy(3, d, n).wait_recv()
             zcopy(4, d, n).start()
+        if n == NC - 1:
+            ystart(1)
         with jax.named_scope(f"hop3w{n}"):
             for d in (0, 1):
                 zcopy(2, d, n).wait_recv()
@@ -545,8 +555,9 @@
         expert_mid(2)
         for n in range(NC):
             expert_out(5, 2, n)
-            for d in (0, 1):
-                rcopy(1, d, n).start()
+            if n < 2:
+                for d in (0, 1):
+                    rcopy(1, d, n).start()
     with jax.named_scope("xw34"):
         xwait(3)
         xwait(4)
@@ -566,18 +577,25 @@
             expert_out(7, 1, n)
             for d in (0, 1):
                 rcopy(0, d, n).start()
-    for n, d in both:
-        with jax.named_scope(f"r3_{n}{d}"):
-            rcopy(1, d, n).wait_recv()
-        exchange(got3, ret3, d, cols_of(n), ssem.at[bs], brecv.at[d, n])
+    def slots3_in(n):
+        for d in (0, 1):
+            with jax.named_scope(f"r3_{n}{d}"):
+                rcopy(1, d, n).wait_recv()
+            exchange(got3, ret3, d, cols_of(n), ssem.at[bs], brecv.at[d, n])
+
+    slots3_in(0)
+    slots3_in(1)
     for n, d in both:
         with jax.named_scope(f"r4_{n}{d}"):
             rcopy(0, d, n).wait_recv()
         rcopy(2, d, n).start()
-    ywait(3)
-    ywait(4)
+        if n < 2:
+            rcopy(1, d, n + 2).start()
 
     def sums2_out(n):
+        if n % 2 == 0:
+            ywait(3, n // 2)
+            ywait(4, n // 2)
         for d in (0, 1):
             with jax.named_scope(f"ex{n}{d}"):
                 wait_bytes(ret3.at[d, 0:others, 0 : cw + hw], brecv.at[d, n])
@@ -593,19 +611,29 @@
             send2[d, :, part_of(n, 1)] = hi.astype(BF)
             rcopy(3, d, n).start()
 
-    for n in range(NC):
+    def slots4_in(n):
         for d in (0, 1):
             with jax.named_scope(f"r3b_{n}{d}"):
                 rcopy(2, d, n).wait_recv()
             exchange(got4, ret4, d, half_of(n), ssem.at[bs], brecv.at[d, n])
-        if n > 0:
-            sums2_out(n - 1)
-    sums2_out(NC - 1)
-    ystart(1)
+
+    slots4_in(0)
+    slots3_in(2)
+    slots4_in(1)
+    ystart(3, 1)
+    ystart(4, 1)
+    sums2_out(0)
+    slots3_in(3)
+    slots4_in(2)
+    sums2_out(1)
+    slots4_in(3)
+    sums2_out(2)
+    sums2_out(3)
     ystart(2)
+    with jax.named_scope("yw12"):
+        ywait(1)
+        ywait(2)
     ystart(0)
-    ywait(1)
-    ywait(2)
     for n, d in both:
         with jax.named_scope(f"r2_{n}{d}"):
             rcopy(3, d, n).wait_recv()
@@ -717,7 +745,7 @@
         ((width, fe), BF),
         ((fe, width), BF),
     ]
-    sems = [(5,), (NC,), (3,), (14,), (3,), (4, NC), (2,), (2, 2), (5, 2, NC), (5,), (5,), (2, NC), (2, NC), (5, 2, NC)]
+    sems = [(5,), (NC,), (3,), (14,), (3,), (4, NC), (2,), (2, 2), (5, 2, NC), (5,), (7,), (2, NC), (2, NC), (5, 2, NC)]
     return pl.pallas_call(
         layer_kernel,
         out_shape=jax.ShapeDtypeStruct((tok, width), BF),

time: 171 us -> 164 us (0.959)
  Pallas kernels: 168 us -> 162 us
    pallas_call x1, Pallas kernels: 168 us -> 162 us  [body(): pl.pallas_call(layer_kernel, out_shape=jax.ShapeDtypeStruct((tok, width),...]
where the time goes in v5:
time: 164 us
  Pallas kernels  162 us (99%)
  local copies, waits for them, and re-layouts  2.3 us (1%)
    pallas_call x1, Pallas kernels, body(): pl.pallas_call(layer_kernel, out_shape=jax.ShapeDtypeStruct((tok, width),...  162 us

profile of v5, /device:TPU:1, one launch (start us, length us, event | category | flops | bytes accessed | tf_op | source)
XLA Modules:
  0.0 164.3 jit_solution(13912591923081065203)
XLA Ops:
  0.0 162.0 %layer.1 = bf16[256,2048]{1,0:T(8,128)(2,1)} custom-call(bf16[256,2048]{1,0:T(8,128)(2,1)} %rin_hbm.1, bf16[1024,256]{1,0:T(8,128)(2,1)} %go_hbm.1, bf16[1024,256]{1,0:T(8,128)(2,1)} %gi_hbm.1, bf16[1024,256]{1,0:T(8,128)(2,1)} %ci_hbm.1, bf16[256,2048]{1,0:T(8,128)(2,1)} %ow_hbm.1, bf16[1,2048,512]{2,1,0:T(8,128)(2,1)} %wg_hbm.1, ...), custom_call_target="tpu_custom_call" | custom-call | tf_op jit(solution)/shard_map/layer/pallas_call | solution.py:749
  162.0 2.3 %copy.16 = bf16[256,2048]{1,0:T(8,128)(2,1)} copy(bf16[256,2048]{1,0:T(8,128)(2,1)} %layer.1) | data formatting | bytes 2097152

commit v6 on v5

--- a/solution.py
+++ b/solution.py
@@ -50,7 +50,6 @@
     gate,
     value,
     mgain,
-    out,
     sel,
     metas,
     hop1,
@@ -82,7 +81,6 @@
     wu,
     wd,
     isem,
-    osem,
     wsem,
     ssem,
     trecv,
@@ -618,9 +616,9 @@
             exchange(got4, ret4, d, half_of(n), ssem.at[bs], brecv.at[d, n])
 
     slots4_in(0)
+    ystart(3, 1)
     slots3_in(2)
     slots4_in(1)
-    ystart(3, 1)
     ystart(4, 1)
     sums2_out(0)
     slots3_in(3)
@@ -628,8 +626,8 @@
     sums2_out(1)
     slots4_in(3)
     sums2_out(2)
+    ystart(2)
     sums2_out(3)
-    ystart(2)
     with jax.named_scope("yw12"):
         ywait(1)
         ywait(2)
@@ -643,7 +641,6 @@
         rcopy(4, d, n).start()
     ywait(0)
     own = spread(0, z)
-    ocopies = []
     for n in range(NC):
         with jax.named_scope(f"r1_{n}"):
             rcopy(4, 0, n).wait_recv()
@@ -651,13 +648,8 @@
         cols = cols_of(n)
         total = res_ref[:, cols].astype(F32) + combine(own, ret0[:, cols])
         total = total + part1[0, :, cols].astype(F32) + part1[1, :, cols].astype(F32)
-        out[:, cols] = total.astype(BF)
-        copy = pltpu.make_async_copy(out.at[:, cols], out_ref.at[:, cols], osem.at[n])
-        copy.start()
-        ocopies.append(copy)
+        out_ref[:, cols] = total.astype(BF)
     with jax.named_scope("ends"):
-        for copy in ocopies:
-            copy.wait()
         flat = ((near_z, 4 * tok), (far_z, 4 * grp), (back_near, 4 * tok), (back_far, 4 * grp), (xs, 5 * others), (ys, 5 * others))
         flat += ((gs, 3 * others), (bs, 3 * others), (ring, 3 * chan), (rows_t, 3 * tok * chan // width), (normed_z, 2 * ntp * tok * chan // width))
         for kind, rows in flat:
@@ -713,7 +705,6 @@
         ((2 * grp, fe), F32),
         ((2 * grp, fe), F32),
         ((8, width), F32),
-        ((tok, width), BF),
         ((5, grp, tok), BF),
         ((NZ, 8, tok), F32),
         ((2, tok, width), BF),
@@ -745,12 +736,12 @@
         ((width, fe), BF),
         ((fe, width), BF),
     ]
-    sems = [(5,), (NC,), (3,), (14,), (3,), (4, NC), (2,), (2, 2), (5, 2, NC), (5,), (7,), (2, NC), (2, NC), (5, 2, NC)]
+    sems = [(5,), (3,), (14,), (3,), (4, NC), (2,), (2, 2), (5, 2, NC), (5,), (7,), (2, NC), (2, NC), (5, 2, NC)]
     return pl.pallas_call(
         layer_kernel,
-        out_shape=jax.ShapeDtypeStruct((tok, width), BF),
+        out_shape=pltpu.VMEM((tok, width), BF),
         in_specs=[hbm] * 8 + [vmem] * 6,
-        out_specs=hbm,
+        out_specs=vmem,
         scratch_shapes=[pltpu.VMEM(s, t) for s, t in shapes] + [dma(s) for s in sems],
         compiler_params=pltpu.CompilerParams(
             collective_id=0, has_side_effects=True, vmem_limit_bytes=61 * 1024 * 1024

time: 164 us -> 162 us (0.988)
  Pallas kernels: 162 us -> 160 us
where the time goes in v6:
time: 162 us; the launch traced here: 161 us
  Pallas kernels  160 us (99%)
    pallas_call x1, Pallas kernels, body(): pl.pallas_call(layer_kernel, out_shape=pltpu.VMEM((tok, width), BF), in_s...  160 us

profile of v6, /device:TPU:1, one launch (start us, length us, event | category | flops | bytes accessed | tf_op | source)
XLA Modules:
  0.0 161.5 jit_solution(17161618617510881014)
XLA Ops:
  0.0 160.5 %layer.1 = bf16[256,2048]{1,0:T(8,128)(2,1)S(1)} custom-call(bf16[256,2048]{1,0:T(8,128)(2,1)} %rin_hbm.1, bf16[1024,256]{1,0:T(8,128)(2,1)} %go_hbm.1, bf16[1024,256]{1,0:T(8,128)(2,1)} %gi_hbm.1, bf16[1024,256]{1,0:T(8,128)(2,1)} %ci_hbm.1, bf16[256,2048]{1,0:T(8,128)(2,1)} %ow_hbm.1, bf16[1,2048,512]{2,1,0:T(8,128)(2,1)} %wg_hbm.1, ...), custom_call_target="tpu_custom_call" | custom-call | tf_op jit(solution)/shard_map/layer/pallas_call | solution.py:740
  160.5 1.0 copy.16

commit v7 on v6

--- a/solution.py
+++ b/solution.py
@@ -23,13 +23,19 @@
     wg_hbm,
     wu_hbm,
     wd_hbm,
+    taps_hbm,
+    gain_hbm,
+    mgain_hbm,
+    ids_hbm,
+    group_hbm,
+    route_hbm,
+    out_ref,
     taps_ref,
     gain_ref,
     mgain_ref,
     ids_ref,
     group_ref,
     route_ref,
-    out_ref,
     rin,
     go,
     gi,
@@ -81,6 +87,7 @@
     wu,
     wd,
     isem,
+    ssmall,
     wsem,
     ssem,
     trecv,
@@ -168,9 +175,12 @@
         meta_ref[3:4, :] = group_ref[...] * route_ref[1:2, :] / (route_ref[0:1, :] + route_ref[1:2, :])
         meta_ref[4:8, :] = jnp.zeros((4, tok), F32)
 
+    smalls = ((ids_hbm, ids_ref), (group_hbm, group_ref), (route_hbm, route_ref))
+    smalls += ((taps_hbm, taps_ref), (gain_hbm, gain_ref), (mgain_hbm, mgain_ref))
+    scopies = [pltpu.make_async_copy(src, dst, ssmall.at[i]) for i, (src, dst) in enumerate(smalls)]
     icopies = [
         pltpu.make_async_copy(src, dst, isem.at[i])
-        for i, (src, dst) in enumerate(((ow_hbm, ow), (rin_hbm, rin), (gi_hbm, gi), (ci_hbm, ci), (go_hbm, go)))
+        for i, (src, dst) in enumerate(((rin_hbm, rin), (ow_hbm, ow), (gi_hbm, gi), (ci_hbm, ci), (go_hbm, go)))
     ]
     wcopies = [
         pltpu.make_async_copy(wg_hbm.at[0], wg, wsem.at[0]),
@@ -186,9 +196,8 @@
         pl.semaphore_signal(barrier, inc=1, device_id=tid(offset), device_id_type=MESH)
     for ident in (after, before):
         pl.semaphore_signal(barrier, inc=1, device_id=ident, device_id_type=MESH)
-    for copy in icopies:
+    for copy in icopies[:2] + scopies + icopies[2:]:
         copy.start()
-    make_slots()
     with jax.named_scope("barrier"):
         pl.semaphore_wait(barrier, nj + ntp + 2)
 
@@ -319,15 +328,19 @@
 
     for i in (0, 1):
         hcopy(i).start()
+    icopies[0].wait()
+    for d in (0, 1):
+        zcopy(0, d, 0).start()
+    icopies[1].wait()
+    for kind in (0, 1):
+        acopy(kind, 0).start()
+    for copy in scopies:
+        copy.wait()
+    with jax.named_scope("slots"):
+        make_slots()
     for d in (0, 1):
         mcopy(0, d).start()
-    with jax.named_scope("inputs"):
-        icopies[0].wait()
-    for kind in (0, 1):
-        acopy(kind, 0).start()
-    with jax.named_scope("rin"):
-        icopies[1].wait()
-    for n in range(NC - 1):
+    for n in range(1, NC - 1):
         for d in (0, 1):
             zcopy(0, d, n).start()
     mgain[...] = jnp.broadcast_to(mgain_ref[...].astype(F32)[None, :], mgain.shape)
@@ -685,6 +698,12 @@
     hbm = pl.BlockSpec(memory_space=pl.ANY)
     dma = pltpu.SemaphoreType.DMA
     shapes = [
+        ((conv_taps.shape[0], chan), BF),
+        ((chan,), BF),
+        ((width,), BF),
+        ((2, tok), jnp.int32),
+        ((1, tok), F32),
+        ((2, tok), F32),
         ((tok, width), BF),
         ((seq, chan), BF),
         ((seq, chan), BF),
@@ -736,11 +755,11 @@
         ((width, fe), BF),
         ((fe, width), BF),
     ]
-    sems = [(5,), (3,), (14,), (3,), (4, NC), (2,), (2, 2), (5, 2, NC), (5,), (7,), (2, NC), (2, NC), (5, 2, NC)]
+    sems = [(5,), (6,), (3,), (14,), (3,), (4, NC), (2,), (2, 2), (5, 2, NC), (5,), (7,), (2, NC), (2, NC), (5, 2, NC)]
     return pl.pallas_call(
         layer_kernel,
         out_shape=pltpu.VMEM((tok, width), BF),
-        in_specs=[hbm] * 8 + [vmem] * 6,
+        in_specs=[hbm] * 14,
         out_specs=vmem,
         scratch_shapes=[pltpu.VMEM(s, t) for s, t in shapes] + [dma(s) for s in sems],
         compiler_params=pltpu.CompilerParams(

time: 162 us -> 161 us (level)
  no operation moved by 1% of the time
where the time goes in v7:
time: 161 us
  Pallas kernels  160 us (99%)
    pallas_call x1, Pallas kernels, body(): pl.pallas_call(layer_kernel, out_shape=pltpu.VMEM((tok, width), BF), in_s...  160 us

profile of v7, /device:TPU:1, one launch (start us, length us, event | category | flops | bytes accessed | tf_op | source)
XLA Modules:
  0.0 160.8 jit_solution(1470534269581915576)
XLA Ops:
  0.0 159.8 %layer.1 = bf16[256,2048]{1,0:T(8,128)(2,1)S(1)} custom-call(bf16[256,2048]{1,0:T(8,128)(2,1)} %rin_hbm.1, bf16[1024,256]{1,0:T(8,128)(2,1)} %go_hbm.1, bf16[1024,256]{1,0:T(8,128)(2,1)} %gi_hbm.1, bf16[1024,256]{1,0:T(8,128)(2,1)} %ci_hbm.1, bf16[256,2048]{1,0:T(8,128)(2,1)} %ow_hbm.1, bf16[1,2048,512]{2,1,0:T(8,128)(2,1)} %wg_hbm.1, ...), custom_call_target="tpu_custom_call" | custom-call | tf_op jit(solution)/shard_map/layer/pallas_call | solution.py:759
  159.8 1.0 copy.16

commit v8 on v7

--- a/solution.py
+++ b/solution.py
@@ -218,7 +218,7 @@
             src, dst = gather4.at[d, :, half_of(n)], pass4.at[d, :, half_of(n)]
         else:
             src, dst = pass4.at[d, :, half_of(n)], arrived.at[block_rows(7), part_of(n, d)]
-        return remote(src, dst, ssem.at[near_z if hop < 2 else far_z], zrecv.at[hop, d, n], zid(step[d]))
+        return remote(src, dst, ssem.at[near_z if hop < 2 else far_z], zrecv.at[(0, 2, 4, 5, 7)[hop] + (0 if hop in (2, 4) else d), n], zid(step[d]))
 
     def meta_of(offset):
         return meta_ref if offset == 0 else metas.at[offset]
@@ -548,7 +548,7 @@
             src, dst = send2.at[d, :, cols], part2.at[d, :, cols]
         else:
             src, dst = send1.at[d, :, cols], part1.at[d, :, cols]
-        return remote(src, dst, ssem.at[back_near if kind > 2 else back_far], rrecv.at[kind, d, n], zid(-step[d]))
+        return remote(src, dst, ssem.at[back_near if kind > 2 else back_far], rrecv.at[8 if kind == 4 else 2 * kind + d, n], zid(-step[d]))
 
     for n in range(NC):
         for d in (0, 1):
@@ -558,8 +558,7 @@
         if n == NC - 1:
             ystart(1)
         with jax.named_scope(f"hop3w{n}"):
-            for d in (0, 1):
-                zcopy(2, d, n).wait_recv()
+            wait_bytes(arrived.at[5 * grp : 7 * grp, cols_of(n)], zrecv.at[4, n])
         with jax.named_scope(f"in56_{n}"):
             expert_in(5, 2, n, n == 0)
     with jax.named_scope("out56"):
@@ -578,8 +577,7 @@
     ystart(4)
     for n in range(NC):
         with jax.named_scope(f"hop4w{n}"):
-            for d in (0, 1):
-                zcopy(4, d, n).wait_recv()
+            wait_bytes(arrived.at[block_rows(7), cols_of(n)], zrecv.at[7, n])
         with jax.named_scope(f"in7_{n}"):
             expert_in(7, 1, n, n == 0)
     with jax.named_scope("out7"):
@@ -646,20 +644,20 @@
         ywait(2)
     ystart(0)
     for n, d in both:
+        cols = cols_of(n)
+        here = combine(spread(near[d], z), ret1[d, :, cols])
         with jax.named_scope(f"r2_{n}{d}"):
             rcopy(3, d, n).wait_recv()
-        cols = cols_of(n)
-        total = part2[d, :, cols].astype(F32) + combine(spread(near[d], z), ret1[d, :, cols])
+        total = part2[d, :, cols].astype(F32) + here
         send1[d, :, cols] = total.astype(BF)
         rcopy(4, d, n).start()
     ywait(0)
     own = spread(0, z)
     for n in range(NC):
-        with jax.named_scope(f"r1_{n}"):
-            rcopy(4, 0, n).wait_recv()
-            rcopy(4, 1, n).wait_recv()
         cols = cols_of(n)
         total = res_ref[:, cols].astype(F32) + combine(own, ret0[:, cols])
+        with jax.named_scope(f"r1_{n}"):
+            wait_bytes(part1.at[:, :, cols], rrecv.at[8, n])
         total = total + part1[0, :, cols].astype(F32) + part1[1, :, cols].astype(F32)
         out_ref[:, cols] = total.astype(BF)
     with jax.named_scope("ends"):
@@ -755,7 +753,7 @@
         ((width, fe), BF),
         ((fe, width), BF),
     ]
-    sems = [(5,), (6,), (3,), (14,), (3,), (4, NC), (2,), (2, 2), (5, 2, NC), (5,), (7,), (2, NC), (2, NC), (5, 2, NC)]
+    sems = [(5,), (6,), (3,), (14,), (3,), (4, NC), (2,), (2, 2), (8, NC), (5,), (7,), (2, NC), (2, NC), (9, NC)]
     return pl.pallas_call(
         layer_kernel,
         out_shape=pltpu.VMEM((tok, width), BF),

time: 161 us -> 161 us (level)
  no operation moved by 1% of the time
where the time goes in v8:
time: 161 us
  Pallas kernels  160 us (99%)
    pallas_call x1, Pallas kernels, body(): pl.pallas_call(layer_kernel, out_shape=pltpu.VMEM((tok, width), BF), in_s...  160 us

profile of v8, /device:TPU:1, one launch (start us, length us, event | category | flops | bytes accessed | tf_op | source)
XLA Modules:
  0.0 160.6 jit_solution(10002080721139879715)
XLA Ops:
  0.0 159.6 %layer.1 = bf16[256,2048]{1,0:T(8,128)(2,1)S(1)} custom-call(bf16[256,2048]{1,0:T(8,128)(2,1)} %rin_hbm.1, bf16[1024,256]{1,0:T(8,128)(2,1)} %go_hbm.1, bf16[1024,256]{1,0:T(8,128)(2,1)} %gi_hbm.1, bf16[1024,256]{1,0:T(8,128)(2,1)} %ci_hbm.1, bf16[256,2048]{1,0:T(8,128)(2,1)} %ow_hbm.1, bf16[1,2048,512]{2,1,0:T(8,128)(2,1)} %wg_hbm.1, ...), custom_call_target="tpu_custom_call" | custom-call | tf_op jit(solution)/shard_map/layer/pallas_call | solution.py:757
  159.6 1.0 copy.16
